TPU v7x, 256 devices: a whole 4x4x8 slice. The times are simulated.
256 devices in a mesh: ep: 64 (over z, y, core), tp: 4 (over x).
Axes of the slice: x: 4, y: 4, z: 8, core: 2. Of those that a mesh axis runs over, the one named last changes fastest.
Arguments:
- tokens: bfloat16 [1024, 2048], P('ep', 'tp'), may hold values from -40 to 40
- kv_cache: bfloat16 [1024, 1024, 512], P('ep', None, 'tp'), may hold values from -1000 to 1000
- cum_gate: float32 [1024, 16, 1024], P('ep', 'tp'), may hold values from -400 to 0, as said below
- lengths: int32 [1024], P('ep'), may hold values from 256 to 1024
- w_query: bfloat16 [2048, 1024], P(None, 'tp'), may hold values from -0.125 to 0.125
- w_key: bfloat16 [2048, 256], P(None, 'tp'), may hold values from -0.125 to 0.125
- w_value: bfloat16 [2048, 256], P(None, 'tp'), may hold values from -0.125 to 0.125
- w_forget: bfloat16 [2048, 16], P(None, 'tp'), may hold values from -0.5 to 0.5
- forget_bias: float32 [16], P('tp'), may hold values from -2.5 to 1.5
- w_out: bfloat16 [1024, 2048], P('tp'), may hold values from -0.1875 to 0.1875
- attn_gain: bfloat16 [2048], replicated, may hold values from 0.099609375 to 1.8984375
- ffn_gain: bfloat16 [2048], replicated, may hold values from 0.099609375 to 1.8984375
- mix_gate: bfloat16 [2048], replicated, may hold values from -0.125 to 0.125
- expert_gate: bfloat16 [64, 2048, 1024], P('ep', None, 'tp'), may hold values from -0.125 to 0.125
- expert_up: bfloat16 [64, 2048, 1024], P('ep', None, 'tp'), may hold values from -0.125 to 0.125
- expert_down: bfloat16 [64, 1024, 2048], P('ep', 'tp'), may hold values from -0.1875 to 0.1875
- chosen: int32 [1024, 2], P('ep'), may hold values from 0 to 63, as said below
- route_weight: float32 [1024, 2], P('ep'), may hold values from 0.5 to 1.5
- dense_gate: bfloat16 [2048, 1024], P(None, 'tp'), may hold values from -0.125 to 0.125
- dense_up: bfloat16 [2048, 1024], P(None, 'tp'), may hold values from -0.125 to 0.125
- dense_down: bfloat16 [1024, 2048], P('tp'), may hold values from -0.1875 to 0.1875
Outputs:
- mixed: bfloat16 [1024, 2048], P('ep', 'tp')
Inputs may be any that keep to these rules, and one draw needn't show every extreme that they name: `cum_gate`: along positions each row never rises: entry p is the sum of the log forget gates of positions 0 to p of that sequence and head. `chosen`: each row names two different experts of one group of 8 consecutive expert numbers. The rows of one device name any one expert at most 2 times, and some expert exactly 2 times.
All inputs are finite; a program needn't handle non-finite values.
Results may differ from a plain program's by a relative error of at most 0.014.
Values may be sent and summed in bfloat16 or wider, within the bound.
A program may use at most 64 MiB of HBM per device.

v0:
```python
import jax
import jax.numpy as jnp
from jax import lax
from jax.sharding import PartitionSpec as P

HD = 64
TOP = 2


epsilon = 1e-06


def copy_for_each(array, axis):
    copies = jnp.broadcast_to(array, (lax.axis_size(axis), *array.shape))
    return lax.all_to_all(copies, axis, split_axis=0, concat_axis=0, tiled=True)


def laid_out(tiles, dim):
    tiles = jnp.moveaxis(tiles, 0, dim)
    shape = tiles.shape
    return tiles.reshape(*shape[:dim], shape[dim] * shape[dim + 1], *shape[dim + 2 :])


def gather_directly(array, axis, dim):
    tiles = copy_for_each(array, axis)
    return laid_out(tiles, dim)


def taken_together(array, axis):
    return copy_for_each(array, axis).astype(jnp.float32).sum(axis=0)


def in_blocks(array, dim, devices):
    before, after = (array.shape[:dim], array.shape[dim + 1 :])
    return jnp.moveaxis(array.reshape(*before, devices, -1, *after), dim, 0)


def sent_and_summed(array, axis, dim):
    tiles = in_blocks(array, dim, lax.axis_size(axis))
    arrived = lax.all_to_all(tiles, axis, split_axis=0, concat_axis=0, tiled=True)
    return arrived.astype(jnp.float32).sum(axis=0)


def norm_rows(values, scales):
    widened = values.astype(jnp.float32)
    square = jnp.mean(widened * widened, axis=-1, keepdims=True)
    return (widened * lax.rsqrt(square + epsilon) * scales.astype(jnp.float32)).astype(jnp.bfloat16)


def attend(h_one, kv_cache, cum_gate, lengths, w_query, w_key, w_value, w_forget, forget_bias):
    tok_count = h_one.shape[0]
    cache_len = kv_cache.shape[1]
    kv_local = w_key.shape[1] // HD
    q_local = w_query.shape[1] // HD
    group_size = q_local // kv_local
    score_scale = HD ** (-0.5)
    queries = jnp.dot(h_one, w_query, preferred_element_type=jnp.float32).astype(jnp.bfloat16)
    queries = queries.reshape(tok_count, kv_local, group_size, HD)
    key_new = jnp.dot(h_one, w_key, preferred_element_type=jnp.float32).astype(jnp.bfloat16)
    key_new = key_new.reshape(tok_count, kv_local, HD)
    value_new = jnp.dot(h_one, w_value, preferred_element_type=jnp.float32).astype(jnp.bfloat16)
    value_new = value_new.reshape(tok_count, kv_local, HD)
    forget_now = jax.nn.log_sigmoid(
        jnp.dot(h_one, w_forget, preferred_element_type=jnp.float32) + forget_bias
    )
    forget_now = forget_now.reshape(tok_count, kv_local, group_size)
    stacked = kv_cache.reshape(tok_count, cache_len, kv_local, 2, HD)
    past_keys = stacked[:, :, :, 0, :]
    past_values = stacked[:, :, :, 1, :]
    scores = (
        jnp.einsum("sjgd,scjd->sjgc", queries, past_keys, preferred_element_type=jnp.float32)
        * score_scale
    )
    cumulative = cum_gate.reshape(tok_count, kv_local, group_size, cache_len)
    position_rows = jnp.arange(cache_len, dtype=jnp.int32)
    at_last = (position_rows[None, :] == (lengths - 1)[:, None]).astype(jnp.float32)
    latest = jnp.sum(cumulative * at_last[:, None, None, :], axis=-1, keepdims=True)
    scores = scores + latest - cumulative + forget_now[:, :, :, None]
    inside = position_rows[None, :] < lengths[:, None]
    scores = jnp.where(inside[:, None, None, :], scores, -jnp.inf)
    own_score = (
        jnp.einsum("sjgd,sjd->sjg", queries, key_new, preferred_element_type=jnp.float32)
        * score_scale
    )
    highest = jnp.maximum(jnp.max(scores, axis=-1), own_score)
    weights = jnp.exp(scores - highest[:, :, :, None])
    own_weight = jnp.exp(own_score - highest)
    denominator = jnp.sum(weights, axis=-1) + own_weight
    weights = (weights / denominator[:, :, :, None]).astype(jnp.bfloat16)
    own_weight = (own_weight / denominator).astype(jnp.bfloat16)
    blended = jnp.einsum(
        "sjgc,scjd->sjgd", weights, past_values, preferred_element_type=jnp.float32
    )
    blended = (
        blended
        + own_weight.astype(jnp.float32)[:, :, :, None]
        * value_new.astype(jnp.float32)[:, :, None, :]
    )
    return blended.astype(jnp.bfloat16).reshape(tok_count, q_local * HD)


def local(
    tokens,
    kv_cache,
    cum_gate,
    lengths,
    w_query,
    w_key,
    w_value,
    w_forget,
    forget_bias,
    w_out,
    attn_gain,
    ffn_gain,
    mix_gate,
    expert_gate,
    expert_up,
    expert_down,
    chosen,
    route_weight,
    dense_gate,
    dense_up,
    dense_down,
):
    tok_count = tokens.shape[0]
    slice_width = tokens.shape[1]
    ep_count = lax.axis_size("ep")
    gathered = gather_directly(tokens, "tp", 1)
    model_width = gathered.shape[1]
    h_one = norm_rows(gathered, attn_gain)
    head_out = attend(
        h_one, kv_cache, cum_gate, lengths, w_query, w_key, w_value, w_forget, forget_bias
    )
    partial_value = jnp.dot(head_out, w_out, preferred_element_type=jnp.float32)
    tp_offset = lax.axis_index("tp") * slice_width
    attention = taken_together(partial_value.astype(jnp.bfloat16), "tp").astype(jnp.float32)
    residual_full = (gathered.astype(jnp.float32) + attention).astype(jnp.bfloat16)
    h_two = norm_rows(residual_full, ffn_gain)
    residual = lax.dynamic_slice_in_dim(residual_full, tp_offset, slice_width, 1)
    capacity = max(2, (4 * tok_count + ep_count - 1) // ep_count)
    routes = chosen.reshape(-1)
    expert_ids = jnp.arange(ep_count, dtype=jnp.int32)
    one_hot = (routes[:, None] == expert_ids[None, :]).astype(jnp.int32)
    rank_of = jnp.sum((jnp.cumsum(one_hot, axis=0) - one_hot) * one_hot, axis=1)
    slot_of = routes * capacity + rank_of
    slot_ids = jnp.arange(ep_count * capacity, dtype=jnp.int32)
    chooser = (slot_ids[:, None] == slot_of[None, :]).astype(jnp.bfloat16)
    per_token = jnp.sum(chooser.reshape(ep_count * capacity, tok_count, TOP), axis=2)
    outgoing = jnp.dot(per_token, h_two, preferred_element_type=jnp.float32).astype(jnp.bfloat16)
    outgoing = outgoing.reshape(ep_count, capacity, model_width)
    received = lax.all_to_all(outgoing, "ep", split_axis=0, concat_axis=0, tiled=True)
    flat_rows = received.reshape(-1, model_width)
    gate_pre = jnp.dot(flat_rows, expert_gate[0], preferred_element_type=jnp.float32)
    up_pre = jnp.dot(flat_rows, expert_up[0], preferred_element_type=jnp.float32)
    hidden = (jax.nn.silu(gate_pre) * up_pre).astype(jnp.bfloat16)
    part_out = jnp.dot(hidden, expert_down[0], preferred_element_type=jnp.float32)
    summed = sent_and_summed(part_out.astype(jnp.bfloat16), "tp", 1)
    shares = summed.astype(jnp.bfloat16).reshape(received.shape[0], received.shape[1], -1)
    returned = lax.all_to_all(shares, "ep", split_axis=0, concat_axis=0, tiled=True)
    returned = returned.reshape(ep_count * capacity, slice_width)
    picked = jnp.dot(chooser.T, returned, preferred_element_type=jnp.float32)
    routed_sum = jnp.sum(
        picked.reshape(tok_count, TOP, slice_width) * route_weight[:, :, None], axis=1
    )
    dense_pre = jnp.dot(h_two, dense_gate, preferred_element_type=jnp.float32)
    dense_lift = jnp.dot(h_two, dense_up, preferred_element_type=jnp.float32)
    dense_act = (jax.nn.silu(dense_pre) * dense_lift).astype(jnp.bfloat16)
    dense_part = jnp.dot(dense_act, dense_down, preferred_element_type=jnp.float32)
    dense_out = sent_and_summed(dense_part.astype(jnp.bfloat16), "tp", 1)
    blend_gate = jax.nn.sigmoid(jnp.dot(h_two, mix_gate, preferred_element_type=jnp.float32))
    return (residual.astype(jnp.float32) + routed_sum + blend_gate[:, None] * dense_out).astype(
        jnp.bfloat16
    )


def solution(mesh):
    in_specs = (
        P("ep", "tp"),
        P("ep", None, "tp"),
        P("ep", "tp", None),
        P("ep"),
        P(None, "tp"),
        P(None, "tp"),
        P(None, "tp"),
        P(None, "tp"),
        P("tp"),
        P("tp", None),
        P(),
        P(),
        P(),
        P("ep", None, "tp"),
        P("ep", None, "tp"),
        P("ep", "tp", None),
        P("ep", None),
        P("ep", None),
        P(None, "tp"),
        P(None, "tp"),
        P("tp", None),
    )
    out_specs = P("ep", "tp")
    return jax.shard_map(local, mesh=mesh, in_specs=in_specs, out_specs=out_specs, check_vma=False)
```

profile of v0, /device:TPU:1, one launch (start us, length us, event | category | flops | bytes accessed | tf_op | source)
XLA Modules:
  0.0 111.3 jit_solution(3181718522928790457)
XLA Ops:
  0.0 1.4 %broadcast_in_dim.12 = bf16[4,16,512]{2,1,0:T(8,128)(2,1)} broadcast(bf16[16,512]{1,0:T(8,128)(2,1)} %param.21), dimensions={1,2} | broadcast | bytes 81920 | tf_op jit(solution)/shard_map/broadcast_in_dim | solution.py:14
  1.4 4.8 %all-to-all-start = ((bf16[4,16,512]{2,1,0:T(8,128)(2,1)}), bf16[4,16,512]{2,1,0:T(8,128)(2,1)S(1)}, u32[]{:S(2)}, u32[]{:S(2)}) async-start(bf16[4,16,512]{2,1,0:T(8,128)(2,1)} %broadcast_in_dim.12), calls=%async_computation | async-start | bytes 131072 | tf_op jit(solution)/shard_map/all_to_all | solution.py:15
  6.3 0.7 broadcast_add_fusion
  6.9 0.8 copy.72
  7.7 0.1 reshape.219
  7.8 0.1 fusion.46
  7.9 0.7 iota_compare_fusion.1
  8.6 0.1 reduce_window_sum.11
  8.7 0.2 select_reduce_fusion
  8.8 0.7 convert_element_type.120
  9.5 0.1 reduce_sum.105
  9.6 0.1 copy.73
  9.7 0.0 copy-start.5
  9.7 0.0 copy-start.2
  9.7 6.5 %copy.68 = bf16[16,1024,128]{1,2,0:T(8,128)(2,1)} copy(bf16[16,1024,128]{2,1,0:T(8,128)(2,1)} %param.22) | data formatting | bytes 8388608 | tf_op args[1]
  16.3 0.0 all-to-all-done
  16.3 0.1 fusion.30
  16.4 0.1 multiply_convert_fusion.1
  16.5 0.2 fusion.14
  16.7 0.1 fusion.55
  16.9 0.1 copy.70
  17.0 0.2 fusion.13
  17.1 0.3 convolution_convert_fusion.4
  17.4 0.1 reshape.214
  17.5 0.1 fusion.51
  17.6 2.1 %fusion.7 = f32[16,4,1024]{2,1,0:T(4,128)S(1)} fusion(bf16[16,4,64]{2,1,0:T(4,128)(2,1)S(1)} %reshape.214, bf16[16,1024,1,2,64]{1,4,3,0,2:T(8,128)(2,1)} %bitcast.95), kind=kOutput, calls=%fused_computation.13 | convolution fusion | flops 8454144 | bytes 2367488 | tf_op jit(solution)/shard_map/sjgd,scjd->sjgc/dot_general | solution.py:71
  19.7 0.0 copy-start.6
  19.7 1.4 %fusion.59 = (f32[16,4]{1,0:T(8,128)S(1)}, f32[16,4,1024]{2,1,0:T(4,128)S(1)}) fusion(f32[16,4]{1,0:T(8,128)S(1)} %copy.70, f32[16,4,1024]{2,1,0:T(4,128)} %param.23, f32[16,4,1024]{2,1,0:T(4,128)S(1)} %fusion.7, f32[16,1024]{1,0:T(8,128)S(1)} %get-tuple-element.10, pred[16,1024]{1,0:T(8,128)(4,1)S(1)} %get-tuple-element.9), kind=kOutput, calls=%fused_computation.101 | output fusion | flops 394239 | bytes 868864 | tf_op jit(solution)/shard_map/add | solution.py:78
  21.1 0.2 fusion.26
  21.4 2.3 %fusion.11 = bf16[16,4,64]{2,1,0:T(4,128)(2,1)S(1)} fusion(bf16[16,1024,1,2,64]{1,4,3,0,2:T(8,128)(2,1)} %bitcast.96, f32[16,4,1024]{2,1,0:T(4,128)S(1)} %get-tuple-element.8, f32[16,4]{1,0:T(8,128)S(1)} %get-tuple-element.6, f32[16,4]{1,0:T(8,128)S(1)} %multiply_maximum_fusion, f32[16,64]{1,0:T(8,128)S(1)} %fusion.13, f32[16,4]{1,0:T(8,128)S(1)} %get-tuple-element.5), kind=kOutput, calls=%fused_computation.19 | convolution fusion | flops 8597504 | bytes 2372352 | tf_op jit(solution)/shard_map/sjgc,scjd->sjgd/dot_general | solution.py:91
  23.7 0.1 reshape.218
  23.8 0.2 convolution_convert_fusion.3
  24.0 0.7 broadcast_in_dim.19
  24.7 4.2 %all-to-all-start.1 = ((bf16[4,16,2048]{2,1,0:T(8,128)(2,1)}), bf16[4,16,2048]{2,1,0:T(8,128)(2,1)S(1)}, u32[]{:S(2)}, u32[]{:S(2)}) async-start(bf16[4,16,2048]{2,1,0:T(8,128)(2,1)} %broadcast_in_dim.19), calls=%async_computation.1 | async-start | bytes 524288 | tf_op jit(solution)/shard_map/all_to_all | solution.py:15
  29.0 0.0 copy-done.8
  29.0 0.1 fusion.49
  29.1 5.4 %all-to-all-done.1 = bf16[4,16,2048]{2,1,0:T(8,128)(2,1)S(1)} async-done(((bf16[4,16,2048]{2,1,0:T(8,128)(2,1)}), bf16[4,16,2048]{2,1,0:T(8,128)(2,1)S(1)}, u32[]{:S(2)}, u32[]{:S(2)}) %all-to-all-start.1) | async-done | bytes 262176 | tf_op jit(solution)/shard_map/all_to_all | solution.py:15
  34.6 0.1 multiply_reduce_fusion.1
  34.7 0.3 convolution_convert_fusion.1
  35.1 1.1 %reshape.220 = bf16[64,2,2048]{2,1,0:T(2,128)(2,1)} reshape(bf16[128,2048]{1,0:T(8,128)(2,1)S(1)} %convolution_convert_fusion.1) | data formatting | bytes 1048576 | tf_op jit(solution)/shard_map/reshape | solution.py:150
  36.2 14.3 %all-to-all-start.2 = ((bf16[64,2,2048]{2,1,0:T(2,128)(2,1)}), bf16[64,2,2048]{2,1,0:T(2,128)(2,1)S(1)}, u32[]{:S(2)}, u32[]{:S(2)}) async-start(bf16[64,2,2048]{2,1,0:T(2,128)(2,1)} %reshape.220), calls=%async_computation.2 | async-start | bytes 1048576 | tf_op jit(solution)/shard_map/all_to_all | solution.py:151
  50.5 17.7 %all-to-all-done.2 = bf16[64,2,2048]{2,1,0:T(2,128)(2,1)S(1)} async-done(((bf16[64,2,2048]{2,1,0:T(2,128)(2,1)}), bf16[64,2,2048]{2,1,0:T(2,128)(2,1)S(1)}, u32[]{:S(2)}, u32[]{:S(2)}) %all-to-all-start.2) | async-done | bytes 524320 | tf_op jit(solution)/shard_map/all_to_all | solution.py:151
  68.2 0.2 reshape.221
  68.4 1.5 %fusion.23 = f32[128,256]{1,0:T(8,128)S(1)} fusion(bf16[128,2048]{1,0:T(8,128)(2,1)S(1)} %reshape.221, bf16[1,2048,256]{2,1,0:T(8,128)(2,1)} %param.34), kind=kOutput, calls=%fused_computation.36 | convolution fusion | flops 134217728 | bytes 1703936 | tf_op jit(solution)/shard_map/dot_general | solution.py:153
  70.0 0.0 copy-start.7
  70.0 0.8 convolution_convert_fusion
  70.8 0.0 copy-start.9
  70.8 0.8 copy.95
  71.6 3.5 %all-to-all-start.3 = ((bf16[4,128,512]{2,1,0:T(8,128)(2,1)}), bf16[4,128,512]{2,1,0:T(8,128)(2,1)S(1)}, u32[]{:S(2)}, u32[]{:S(2)}) async-start(bf16[4,128,512]{2,1,0:T(8,128)(2,1)} %bitcast.92), calls=%async_computation.3 | async-start | bytes 1048576 | tf_op jit(solution)/shard_map/all_to_all | solution.py:40
  75.1 1.5 %fusion.58 = f32[16,256]{1,0:T(8,128)S(1)} fusion(bf16[2048,256]{1,0:T(8,128)(2,1)} %param.39, bf16[16,2048]{1,0:T(8,128)(2,1)S(1)} %add_convert_fusion, f32[2048]{0:T(1024)S(1)} %convert_element_type.140, f32[16]{0:T(128)S(1)} %add_rsqrt_fusion), kind=kOutput, calls=%fused_computation.100 | convolution fusion | flops 16908288 | bytes 1138752 | tf_op jit(solution)/shard_map/dot_general | solution.py:165
  76.6 2.3 %convolution_convert_fusion.2 = bf16[16,2048]{1,0:T(8,128)(2,1)S(1)} fusion(bf16[256,2048]{1,0:T(8,128)(2,1)} %param.41, bf16[2048,256]{1,0:T(8,128)(2,1)} %param.40, f32[16,256]{1,0:T(8,128)S(1)} %fusion.58, bf16[16,2048]{1,0:T(8,128)(2,1)S(1)} %add_convert_fusion, f32[2048]{0:T(1024)S(1)} %convert_element_type.140, f32[16]{0:T(128)S(1)} %add_rsqrt_fusion), kind=kOutput, calls=%fused_computation.3 | convolution fusion | flops 33742848 | bytes 2252864 | tf_op jit(solution)/shard_map/dot_general | solution.py:168
  78.9 0.6 copy.96
  79.6 4.7 %all-to-all-done.3 = bf16[4,128,512]{2,1,0:T(8,128)(2,1)S(1)} async-done(((bf16[4,128,512]{2,1,0:T(8,128)(2,1)}), bf16[4,128,512]{2,1,0:T(8,128)(2,1)S(1)}, u32[]{:S(2)}, u32[]{:S(2)}) %all-to-all-start.3) | async-done | bytes 524320 | tf_op jit(solution)/shard_map/all_to_all | solution.py:40
  84.2 3.3 %all-to-all-start.5 = ((bf16[4,16,512]{2,1,0:T(8,128)(2,1)}), bf16[4,16,512]{2,1,0:T(8,128)(2,1)S(1)}, u32[]{:S(2)}, u32[]{:S(2)}) async-start(bf16[4,16,512]{2,1,0:T(8,128)(2,1)} %bitcast.94), calls=%async_computation.5 | async-start | bytes 131072 | tf_op jit(solution)/shard_map/all_to_all | solution.py:40
  87.5 0.1 iota_compare_fusion.4
  87.6 0.1 reduce_sum.109
  87.7 0.7 reshape.223
  88.4 3.6 %all-to-all-done.5 = bf16[4,16,512]{2,1,0:T(8,128)(2,1)S(1)} async-done(((bf16[4,16,512]{2,1,0:T(8,128)(2,1)}), bf16[4,16,512]{2,1,0:T(8,128)(2,1)S(1)}, u32[]{:S(2)}, u32[]{:S(2)}) %all-to-all-start.5) | async-done | bytes 65568 | tf_op jit(solution)/shard_map/all_to_all | solution.py:40
  92.0 7.3 %all-to-all-start.4 = ((bf16[64,2,512]{2,1,0:T(2,128)(2,1)}), bf16[64,2,512]{2,1,0:T(2,128)(2,1)S(1)}, u32[]{:S(2)}, u32[]{:S(2)}) async-start(bf16[64,2,512]{2,1,0:T(2,128)(2,1)} %reshape.223), calls=%async_computation.4 | async-start | bytes 262144 | tf_op jit(solution)/shard_map/all_to_all | solution.py:159
  99.3 0.2 fusion.19
  99.6 10.9 %all-to-all-done.4 = bf16[64,2,512]{2,1,0:T(2,128)(2,1)S(1)} async-done(((bf16[64,2,512]{2,1,0:T(2,128)(2,1)}), bf16[64,2,512]{2,1,0:T(2,128)(2,1)S(1)}, u32[]{:S(2)}, u32[]{:S(2)}) %all-to-all-start.4) | async-done | bytes 131104 | tf_op jit(solution)/shard_map/all_to_all | solution.py:159
  110.4 0.1 reshape.229
  110.5 0.1 fusion.9
  110.6 0.7 add_convert_fusion.1
  (32 shorter events, 0.2 us)
Async XLA Ops:
  0.0 70.0 %copy-start = (bf16[1,256,2048]{2,1,0:T(8,128)(2,1)S(1)}, bf16[1,256,2048]{2,1,0:T(8,128)(2,1)}, u32[]{:S(2)}) copy-start(bf16[1,256,2048]{2,1,0:T(8,128)(2,1)} %param.36) | copy-start | bytes 3145732
  1.4 14.8 %all-to-all-start = ((bf16[4,16,512]{2,1,0:T(8,128)(2,1)}), bf16[4,16,512]{2,1,0:T(8,128)(2,1)S(1)}, u32[]{:S(2)}, u32[]{:S(2)}) async-start(bf16[4,16,512]{2,1,0:T(8,128)(2,1)} %broadcast_in_dim.12), calls=%async_computation | async-start | bytes 131072 | tf_op jit(solution)/shard_map/all_to_all | solution.py:15
  9.7 6.8 %copy-start.4 = (bf16[2048,64]{0,1:T(8,128)(2,1)S(1)}, bf16[2048,64]{0,1:T(8,128)(2,1)}, u32[]{:S(2)}) copy-start(bf16[2048,64]{0,1:T(8,128)(2,1)} %param.26) | copy-start | bytes 786436
  9.7 7.0 %copy-start.10 = (bf16[2048,4]{0,1:T(4,128)(2,1)S(1)}, bf16[2048,4]{0,1:T(4,128)(2,1)}, u32[]{:S(2)}) copy-start(bf16[2048,4]{0,1:T(4,128)(2,1)} %param.28) | copy-start | bytes 49156
  9.7 7.0 %copy-start.11 = (f32[4]{0:T(128)S(1)}, f32[4]{0:T(128)}, u32[]{:S(2)}) copy-start(f32[4]{0:T(128)} %param.29) | copy-start | bytes 52
  9.7 7.3 %copy-start.5 = (bf16[2048,64]{0,1:T(8,128)(2,1)S(1)}, bf16[2048,64]{0,1:T(8,128)(2,1)}, u32[]{:S(2)}) copy-start(bf16[2048,64]{0,1:T(8,128)(2,1)} %param.27) | copy-start | bytes 786436
  9.7 7.4 %copy-start.2 = (bf16[2048,256]{1,0:T(8,128)(2,1)S(1)}, bf16[2048,256]{1,0:T(8,128)(2,1)}, u32[]{:S(2)}) copy-start(bf16[2048,256]{1,0:T(8,128)(2,1)} %param.25) | copy-start | bytes 3145732
  17.4 6.4 %copy-start.3 = (bf16[256,2048]{1,0:T(8,128)(2,1)S(1)}, bf16[256,2048]{1,0:T(8,128)(2,1)}, u32[]{:S(2)}) copy-start(bf16[256,2048]{1,0:T(8,128)(2,1)} %param.30) | copy-start | bytes 3145732
  19.7 9.3 %copy-start.8 = (s32[16,2]{0,1:T(2,128)S(1)}, s32[16,2]{0,1:T(2,128)}, u32[]{:S(2)}) copy-start(s32[16,2]{0,1:T(2,128)} %param.37) | copy-start | bytes 388
  19.7 9.3 %copy-start.6 = (bf16[2048]{0:T(1024)(128)(2,1)S(1)}, bf16[2048]{0:T(1024)(128)(2,1)}, u32[]{:S(2)}) copy-start(bf16[2048]{0:T(1024)(128)(2,1)} %param.32) | copy-start | bytes 12292
  23.7 46.3 %copy-start.1 = (bf16[1,2048,256]{2,1,0:T(8,128)(2,1)S(1)}, bf16[1,2048,256]{2,1,0:T(8,128)(2,1)}, u32[]{:S(2)}) copy-start(bf16[1,2048,256]{2,1,0:T(8,128)(2,1)} %param.35) | copy-start | bytes 3145732
  24.7 9.8 %all-to-all-start.1 = ((bf16[4,16,2048]{2,1,0:T(8,128)(2,1)}), bf16[4,16,2048]{2,1,0:T(8,128)(2,1)S(1)}, u32[]{:S(2)}, u32[]{:S(2)}) async-start(bf16[4,16,2048]{2,1,0:T(8,128)(2,1)} %broadcast_in_dim.19), calls=%async_computation.1 | async-start | bytes 524288 | tf_op jit(solution)/shard_map/all_to_all | solution.py:15
  36.2 32.0 %all-to-all-start.2 = ((bf16[64,2,2048]{2,1,0:T(2,128)(2,1)}), bf16[64,2,2048]{2,1,0:T(2,128)(2,1)S(1)}, u32[]{:S(2)}, u32[]{:S(2)}) async-start(bf16[64,2,2048]{2,1,0:T(2,128)(2,1)} %reshape.220), calls=%async_computation.2 | async-start | bytes 1048576 | tf_op jit(solution)/shard_map/all_to_all | solution.py:151
  70.0 17.6 %copy-start.7 = (bf16[2048]{0:T(1024)(128)(2,1)S(1)}, bf16[2048]{0:T(1024)(128)(2,1)}, u32[]{:S(2)}) copy-start(bf16[2048]{0:T(1024)(128)(2,1)} %param.33) | copy-start | bytes 12292
  70.8 39.7 %copy-start.9 = (f32[16,2]{0,1:T(2,128)S(1)}, f32[16,2]{0,1:T(2,128)}, u32[]{:S(2)}) copy-start(f32[16,2]{0,1:T(2,128)} %param.38) | copy-start | bytes 388
  71.6 12.6 %all-to-all-start.3 = ((bf16[4,128,512]{2,1,0:T(8,128)(2,1)}), bf16[4,128,512]{2,1,0:T(8,128)(2,1)S(1)}, u32[]{:S(2)}, u32[]{:S(2)}) async-start(bf16[4,128,512]{2,1,0:T(8,128)(2,1)} %bitcast.92), calls=%async_computation.3 | async-start | bytes 1048576 | tf_op jit(solution)/shard_map/all_to_all | solution.py:40
  84.2 7.7 %all-to-all-start.5 = ((bf16[4,16,512]{2,1,0:T(8,128)(2,1)}), bf16[4,16,512]{2,1,0:T(8,128)(2,1)S(1)}, u32[]{:S(2)}, u32[]{:S(2)}) async-start(bf16[4,16,512]{2,1,0:T(8,128)(2,1)} %bitcast.94), calls=%async_computation.5 | async-start | bytes 131072 | tf_op jit(solution)/shard_map/all_to_all | solution.py:40
  92.0 18.4 %all-to-all-start.4 = ((bf16[64,2,512]{2,1,0:T(2,128)(2,1)}), bf16[64,2,512]{2,1,0:T(2,128)(2,1)S(1)}, u32[]{:S(2)}, u32[]{:S(2)}) async-start(bf16[64,2,512]{2,1,0:T(2,128)(2,1)} %reshape.223), calls=%async_computation.4 | async-start | bytes 262144 | tf_op jit(solution)/shard_map/all_to_all | solution.py:159
where the time goes:
time: 112 us; the launch traced here: 111 us
  waiting for transfers between devices  42.2 us (38%)
  starting transfers between devices  37.5 us (33%)
  local copies, waits for them, and re-layouts  13.6 us (12%)
  matrix products  12.3 us (11%)
  other arithmetic  5.45 us (5%)
    all_to_all x1, waiting for transfers between devices, local(): lax.all_to_all(outgoing, 'ep', split_axis=0, concat_axis=0, tiled=True)  17.7 us
    all_to_all x1, starting transfers between devices, local(): lax.all_to_all(outgoing, 'ep', split_axis=0, concat_axis=0, tiled=True)  14.3 us
    all_to_all x1, waiting for transfers between devices, local(): lax.all_to_all(shares, 'ep', split_axis=0, concat_axis=0, tiled=True)  10.9 us
    all_to_all x2, starting transfers between devices, copy_for_each(): return lax.all_to_all(copies, axis, split_axis=0, concat_axis=0, tiled=True)  9.07 us
    all_to_all x2, waiting for transfers between devices, sent_and_summed(): lax.all_to_all(tiles, axis, split_axis=0, concat_axis=0, tiled=True)  8.24 us
    unnamed x27, local copies, waits for them, and re-layouts  7.34 us
    all_to_all x1, starting transfers between devices, local(): lax.all_to_all(shares, 'ep', split_axis=0, concat_axis=0, tiled=True)  7.33 us
    all_to_all x2, starting transfers between devices, sent_and_summed(): lax.all_to_all(tiles, axis, split_axis=0, concat_axis=0, tiled=True)  6.75 us
  transfers between devices with their start and end apart: 6, of which 5 were waited for; matrix products, arithmetic and copies ran while one was open for 14% of the time, Pallas kernels for 0%

commit v1 on v0

v1 whole, which is shorter than its diff:
```python
import jax
import jax.numpy as jnp
from jax import lax
from jax.experimental import pallas as pl
from jax.experimental.pallas import tpu as pltpu
from jax.sharding import PartitionSpec as P

EPS = 1e-06
F32 = jnp.float32
BF16 = jnp.bfloat16
MESH = pl.DeviceIdType.MESH
ANY = pl.ANY

TOK = 16
HD = 64
NTP = 4
NZ = 8
NR = 8
NEP = 64
W = 512
NT = (((1,), (1,)), ((), ()))


def iota(shape, dim):
    return lax.broadcasted_iota(jnp.int32, shape, dim)


def dot(a, b):
    return jnp.dot(a, b, preferred_element_type=F32)


def dot_nt(a, b):
    return lax.dot_general(a, b, NT, preferred_element_type=F32)


def one_hot(mask):
    return jnp.where(mask, 1.0, 0.0).astype(BF16)


def three_parts(a):
    hi = a.astype(BF16)
    rest = a - hi.astype(F32)
    mid = rest.astype(BF16)
    low = (rest - mid.astype(F32)).astype(BF16)
    return hi, mid, low


def gain_row(gain_ref):
    gain = gain_ref[...].astype(F32)
    return jnp.concatenate([gain[j : j + 1, :] for j in range(16)], axis=1)


def silu(a):
    return a * (1.0 / (1.0 + jnp.exp(-a)))


def layer(
    tokens,
    lengths,
    forget_bias,
    attn_gain,
    ffn_gain,
    mix_gate,
    chosen,
    route_weight,
    kv_hbm,
    cum_hbm,
    wq_hbm,
    wk_hbm,
    wv_hbm,
    wf_hbm,
    wo_hbm,
    eg_hbm,
    eu_hbm,
    ed_hbm,
    dg_hbm,
    du_hbm,
    dd_hbm,
    out,
    kv,
    cum,
    wq,
    wkv,
    wf,
    wo,
    eg,
    eu,
    ed,
    dg,
    du,
    dd,
    xbuf,
    gate,
    q2,
    sc,
    ob,
    pbuf,
    abuf,
    dmat,
    rmat,
    perm,
    permt,
    resb,
    rbuf,
    outg,
    gath,
    hbuf,
    dsend,
    dbuf,
    ysend,
    ybuf,
    rout,
    rin,
    ffn32,
    load_sem,
    kv_sem,
    x_send,
    x_recv,
    ready_a,
    ready_b,
    p_send,
    p_recv,
    r_send,
    r_recv,
    o_send,
    o_recv,
    g_send,
    g_recv,
    d_send,
    d_recv,
    y_send,
    y_recv,
    b_send,
    b_recv,
):
    ep = lax.axis_index("ep")
    tp = lax.axis_index("tp")
    z = ep // NR
    r = ep % NR
    peers = [(tp + i) % NTP for i in (2, 1, 3)]

    def load(src, dst, i):
        copy = pltpu.make_async_copy(src, dst, load_sem.at[i])
        copy.start()
        return copy

    def remote(src, dst, send, recv, device):
        return pltpu.make_async_remote_copy(
            src_ref=src,
            dst_ref=dst,
            send_sem=send,
            recv_sem=recv,
            device_id=device,
            device_id_type=MESH,
        )

    def arrived(ref, sem):
        remote(ref, ref, x_send, sem, {"tp": peers[0]}).wait_recv()

    def left(ref, sem):
        remote(ref, ref, sem, x_recv.at[0], {"tp": peers[0]}).wait_send()

    barrier = pltpu.get_barrier_semaphore()
    for p in peers:
        pl.semaphore_signal(barrier, inc=1, device_id={"tp": p}, device_id_type=MESH)
    for i in range(1, NR):
        pl.semaphore_signal(
            barrier, inc=1, device_id={"ep": z * NR + (r + i) % NR}, device_id_type=MESH
        )
    for i in (1, 2, 6, 7):
        pl.semaphore_signal(
            barrier, inc=1, device_id={"ep": ((z + i) % NZ) * NR + r}, device_id_type=MESH
        )

    loads = {}
    loads["cum"] = load(cum_hbm, cum, 0)
    loads["wk"] = load(wk_hbm, wkv.at[pl.ds(0, 64)], 1)
    loads["wv"] = load(wv_hbm, wkv.at[pl.ds(64, 64)], 2)
    loads["wf"] = load(wf_hbm, wf, 3)
    loads["wq"] = load(wq_hbm, wq, 4)
    kv_loads = []
    for p in range(8):
        copy = pltpu.make_async_copy(
            kv_hbm.at[pl.ds(2 * p, 2)], kv.at[pl.ds(2 * p, 2)], kv_sem.at[p]
        )
        copy.start()
        kv_loads.append(copy)
    loads["wo"] = load(wo_hbm, wo, 5)
    loads["dg"] = load(dg_hbm, dg, 6)
    loads["du"] = load(du_hbm, du, 7)
    loads["dd"] = load(dd_hbm, dd, 8)
    loads["eg"] = load(eg_hbm, eg, 9)
    loads["eu"] = load(eu_hbm, eu, 10)
    loads["ed"] = load(ed_hbm, ed, 11)

    pl.semaphore_wait(barrier, 14)

    for p in peers:
        remote(tokens, xbuf.at[tp], x_send, x_recv.at[tp], {"tp": p}).start()
    for i in (2, 6):
        pl.semaphore_signal(
            ready_a, inc=1, device_id={"ep": ((z + i) % NZ) * NR + r}, device_id_type=MESH
        )
    xbuf[tp] = tokens[...]
    ffn32[...] = ffn_gain[...].astype(F32)

    loads["cum"].wait()

    def gate_pair(p, carry):
        both = jnp.concatenate([cum[2 * p], cum[2 * p + 1]], axis=0)
        row = iota((8, 1024), 0)
        pos = iota((8, 1024), 1)
        length = jnp.where(row < 4, lengths[2 * p], lengths[2 * p + 1])
        last = jnp.sum(jnp.where(pos == length - 1, both, 0.0), axis=1, keepdims=True)
        gate[pl.ds(pl.multiple_of(8 * p, 8), 8), :] = jnp.where(
            pos < length, last - both, -jnp.inf
        )
        return carry

    lax.fori_loop(0, 8, gate_pair, 0)

    pl.semaphore_wait(ready_a, 2)
    for i in range(1, NR):
        pl.semaphore_signal(
            ready_b, inc=1, device_id={"ep": z * NR + (r + i) % NR}, device_id_type=MESH
        )

    pick = chosen[...]
    expert = iota((NEP, TOK), 0)
    hot = [jnp.where(expert == pick[k : k + 1, :], 1.0, 0.0) for k in range(2)]
    earlier = one_hot(iota((TOK, TOK), 0) < iota((TOK, TOK), 1))
    before = dot((hot[0] + hot[1]).astype(BF16), earlier)
    slots = [
        2.0 * pick[k : k + 1, :].astype(F32) + jnp.sum(hot[k] * before, axis=0, keepdims=True)
        for k in range(2)
    ]
    weight = route_weight[...]
    w_rows = [three_parts(weight[k : k + 1, :]) for k in range(2)]
    info = jnp.concatenate(
        slots + [part.astype(F32) for k in range(2) for part in w_rows[k]], axis=0
    ).astype(BF16)
    spread = one_hot(iota((TOK, 64), 0) == iota((TOK, 64), 1) % TOK)
    spread_t = one_hot(iota((64, TOK), 0) % TOK == iota((64, TOK), 1))
    info_rows = dot(info, spread).astype(jnp.int32)
    info_cols = dot_nt(spread_t, info)
    row = iota((512, 64), 0)
    col_fb = iota((512, 64), 1) // TOK
    dmask = jnp.zeros((512, 64), F32)
    for k in range(2):
        dmask = dmask + jnp.where(row == info_rows[k : k + 1, :] * 4 + col_fb, 1.0, 0.0)
    dmat[...] = dmask.astype(BF16)
    lane = iota((64, 512), 1)
    row_fb = iota((64, 512), 0) // TOK
    for k in range(2):
        slot_col = info_cols[:, k : k + 1].astype(jnp.int32)
        rmat[pl.ds(64 * k, 64), :] = one_hot(lane == slot_col * 4 + row_fb)
    w_cols = [
        info_cols[:, 2 + 3 * k : 3 + 3 * k]
        + info_cols[:, 3 + 3 * k : 4 + 3 * k]
        + info_cols[:, 4 + 3 * k : 5 + 3 * k]
        for k in range(2)
    ]

    def perm_part(i, carry):
        base = pl.multiple_of(64 * i, 64)
        a = iota((64, 512), 0) + base
        b = iota((64, 512), 1)
        perm[pl.ds(base, 64), :] = one_hot((a % 128) * 4 + a // 128 == b)
        permt[pl.ds(base, 64), :] = one_hot((b % 128) * 4 + b // 128 == a)
        return carry

    lax.fori_loop(0, 8, perm_part, 0)

    for p in peers:
        arrived(xbuf.at[p], x_recv.at[p])
    x_full = jnp.concatenate([xbuf[p] for p in range(NTP)], axis=1).astype(F32)
    square = jnp.mean(x_full * x_full, axis=1, keepdims=True)
    h_one = (x_full * lax.rsqrt(square + EPS) * gain_row(attn_gain)).astype(BF16)

    for name in ("wk", "wv", "wf", "wq"):
        loads[name].wait()
    query = dot(h_one, wq[...]).astype(BF16)
    kv_new = dot_nt(h_one, wkv[...]).astype(BF16)
    forget = dot_nt(h_one, wf[...])
    head_lane = iota((TOK, 4), 1)
    bias = jnp.zeros((TOK, 4), F32)
    for h in range(4):
        bias = jnp.where(head_lane == h, forget_bias[h], bias)
    forget = forget + bias
    forget = jnp.minimum(forget, 0.0) - jnp.log1p(jnp.exp(-jnp.abs(forget)))

    row64 = iota((64, TOK), 0)
    col16 = iota((64, TOK), 1)
    repeat = one_hot(row64 // 4 == col16)
    row32 = iota((64, 32), 0)
    col32 = iota((64, 32), 1)
    even = one_hot((row32 // 4 == col32 % TOK) & (row32 % 4 == (col32 // TOK) * 2))
    odd = one_hot((row32 // 4 == col32 % TOK) & (row32 % 4 == (col32 // TOK) * 2 + 1))
    stacked = jnp.concatenate([query[:, 0:128], query[:, 128:256]], axis=0)
    low_half = iota((64, 128), 1) < HD
    q64 = jnp.where(
        low_half, dot(even, stacked) + pltpu.roll(dot(odd, stacked), HD, 1), 0.0
    )
    kv64 = dot(repeat, kv_new)
    f_parts = three_parts(forget)
    f64 = dot(repeat, f_parts[0]) + dot(repeat, f_parts[1]) + dot(repeat, f_parts[2])
    f64 = jnp.sum(
        jnp.where(iota((64, 4), 0) % 4 == iota((64, 4), 1), f64, 0.0), axis=1, keepdims=True
    )
    scale = HD ** (-0.5)
    own = jnp.sum(q64 * kv64, axis=1, keepdims=True) * scale - f64
    first = iota((64, 128), 0) % 8 < 4
    q2[:, 0:128] = jnp.where(first, q64, 0.0)
    q2[:, 128:256] = jnp.where(first, 0.0, q64)

    for p in range(8):
        kv_loads[p].wait()
        keys = jnp.concatenate([kv[2 * p], kv[2 * p + 1]], axis=1)
        sc[pl.ds(8 * p, 8), :] = dot_nt(q2[pl.ds(8 * p, 8), :].astype(BF16), keys)
    score = sc[...] * scale + gate[...]
    highest = jnp.maximum(jnp.max(score, axis=1, keepdims=True), own)
    prob = jnp.exp(score - highest)
    own_prob = jnp.exp(own - highest)
    total = jnp.sum(prob, axis=1, keepdims=True) + own_prob
    inverse = 1.0 / total
    sc[...] = prob * inverse
    own_prob = own_prob * inverse
    for p in range(8):
        values = jnp.concatenate([kv[2 * p], kv[2 * p + 1]], axis=1)
        ob[pl.ds(8 * p, 8), :] = dot(sc[pl.ds(8 * p, 8), :].astype(BF16), values)
    blended = jnp.where(first, ob[:, 0:128], ob[:, 128:256])
    blended = (blended + own_prob.astype(BF16).astype(F32) * kv64).astype(BF16)
    back = one_hot(
        iota((64, 64), 1) == (iota((64, 64), 0) % TOK) * 4 + iota((64, 64), 0) // TOK
    )
    heads = dot(back, blended)
    low16 = iota((TOK, 128), 1) < HD
    head_out = jnp.concatenate(
        [
            jnp.where(low16, pltpu.roll(heads[0:16], HD, 1), heads[16:32]),
            jnp.where(low16, pltpu.roll(heads[32:48], HD, 1), heads[48:64]),
        ],
        axis=1,
    ).astype(BF16)
    loads["wo"].wait()
    partial = dot(head_out, wo[...]).astype(BF16)
    for p in range(NTP):
        pbuf[p] = partial[:, p * W : (p + 1) * W]
    for p in peers:
        remote(pbuf.at[p], abuf.at[tp], p_send, p_recv.at[tp], {"tp": p}).start()
    abuf[tp] = pbuf[tp]

    pl.semaphore_wait(ready_b, 7)

    for p in peers:
        arrived(abuf.at[p], p_recv.at[p])
    attention = abuf[0].astype(F32)
    for p in range(1, NTP):
        attention = attention + abuf[p].astype(F32)
    residual = (tokens[...].astype(F32) + attention).astype(BF16)
    resb[...] = residual
    stacked = jnp.concatenate([residual[:, f * 128 : (f + 1) * 128] for f in range(4)], axis=0)
    outgoing = dot(dmat[...], stacked)
    outg[...] = outgoing.reshape(NEP, 8, 128).astype(BF16)

    def send_out(i, carry):
        k = i // NR
        dz = jnp.where(k % 2 == 1, 4 - (k + 1) // 2, (4 + k // 2) % 8)
        dr = (r + i + 1) % NR
        e = ((z + dz) % NZ) * NR + dr
        remote(outg.at[e], gath.at[tp, ep], o_send, o_recv.at[z], {"ep": e}).start()
        return carry

    lax.fori_loop(0, 63, send_out, 0)
    gath[tp, ep] = outg[ep]
    for p in peers:
        remote(resb, rbuf.at[tp], r_send, r_recv.at[tp], {"tp": p}).start()
    rbuf[tp] = resb[...]

    for dz in (0, 1, 7, 2, 6, 3, 5, 4):
        src_z = (z + dz) % NZ
        base = src_z * NR
        count = NR - 1 if dz == 0 else NR
        arrived(gath.at[tp, pl.ds(base, count)], o_recv.at[src_z])
        chunk = gath.at[tp, pl.ds(base, NR)]
        for p in peers:
            remote(chunk, chunk, g_send, g_recv.at[tp], {"tp": p}).start()

    for p in peers:
        arrived(rbuf.at[p], r_recv.at[p])
    res_full = jnp.concatenate([rbuf[p] for p in range(NTP)], axis=1).astype(F32)
    square = jnp.mean(res_full * res_full, axis=1, keepdims=True)
    ffn_row = gain_row(ffn_gain)
    h_two = (res_full * lax.rsqrt(square + EPS) * ffn_row).astype(BF16)
    for name in ("dg", "du", "dd"):
        loads[name].wait()
    dense_act = (silu(dot(h_two, dg[...])) * dot(h_two, du[...])).astype(BF16)
    dense_part = dot(dense_act, dd[...]).astype(BF16)
    for p in range(NTP):
        dsend[p] = dense_part[:, p * W : (p + 1) * W]
    for p in peers:
        remote(dsend.at[p], dbuf.at[tp], d_send, d_recv.at[tp], {"tp": p}).start()
    dbuf[tp] = dsend[tp]
    mixing = jnp.sum(h_two.astype(F32) * gain_row(mix_gate), axis=1, keepdims=True)
    blend = 1.0 / (1.0 + jnp.exp(-mixing))

    for name in ("eg", "eu", "ed"):
        loads[name].wait()
    squares = jnp.zeros((128, 128), F32)
    for i in (0, 1, 3, 2):
        p = (tp + i) % NTP
        if i:
            arrived(gath.at[p], g_recv.at[p])
        rows = dot(perm[...], gath[p].reshape(512, 128))
        for f in range(4):
            block = rows[128 * f : 128 * f + 128]
            squares = squares + block * block
            c = p * 4 + f
            scaled = block * ffn32[pl.ds(c, 1), :]
            hbuf[:, pl.ds(pl.multiple_of(c * 128, 128), 128)] = scaled.astype(BF16)
    root = lax.rsqrt(jnp.sum(squares, axis=1, keepdims=True) * (1.0 / 2048.0) + EPS)
    hidden = hbuf[...]
    gate_pre = dot(hidden, eg[...]) * root
    up_pre = dot(hidden, eu[...]) * root
    act = (silu(gate_pre) * up_pre).astype(BF16)
    for p in peers:
        ysend[p] = dot(act, ed[:, pl.ds(pl.multiple_of(p * W, W), W)]).astype(BF16)
        remote(ysend.at[p], ybuf.at[tp], y_send, y_recv.at[tp], {"tp": p}).start()
    summed = dot(act, ed[:, pl.ds(pl.multiple_of(tp * W, W), W)]).astype(BF16).astype(F32)
    for p in peers:
        arrived(ybuf.at[p], y_recv.at[p])
        summed = summed + ybuf[p].astype(F32)
    summed = summed.astype(BF16)
    stacked = jnp.concatenate([summed[:, f * 128 : (f + 1) * 128] for f in range(4)], axis=0)
    rout[...] = dot(permt[...], stacked).reshape(NEP, 8, 128).astype(BF16)

    def send_back(i, carry):
        k = i // NR
        dz = jnp.where(k % 2 == 1, 4 - (k + 1) // 2, (4 + k // 2) % 8)
        dr = (r + i + 1) % NR
        e = ((z + dz) % NZ) * NR + dr
        remote(rout.at[e], rin.at[ep], b_send, b_recv, {"ep": e}).start()
        return carry

    lax.fori_loop(0, 63, send_back, 0)
    rin[ep] = rout[ep]

    for p in peers:
        arrived(dbuf.at[p], d_recv.at[p])
    dense_out = dbuf[0].astype(F32)
    for p in range(1, NTP):
        dense_out = dense_out + dbuf[p].astype(F32)
    mixed = residual.astype(F32) + blend * dense_out

    arrived(rin.at[pl.ds(0, 63)], b_recv)
    picked = dot(rmat[...], rin[...].reshape(512, 128))
    routed = picked[0:64] * w_cols[0] + picked[64:128] * w_cols[1]
    routed = jnp.concatenate([routed[16 * f : 16 * f + 16] for f in range(4)], axis=1)
    out[...] = (mixed + routed).astype(BF16)

    left(xbuf.at[pl.ds(0, 3)], x_send)
    left(pbuf.at[pl.ds(0, 3)], p_send)
    left(rbuf.at[pl.ds(0, 3)], r_send)
    left(outg.at[pl.ds(0, 63)], o_send)
    left(gath.at[pl.ds(0, 3)], g_send)
    left(dsend.at[pl.ds(0, 3)], d_send)
    left(ysend.at[pl.ds(0, 3)], y_send)
    left(rout.at[pl.ds(0, 63)], b_send)


def local(
    tokens,
    kv_cache,
    cum_gate,
    lengths,
    w_query,
    w_key,
    w_value,
    w_forget,
    forget_bias,
    w_out,
    attn_gain,
    ffn_gain,
    mix_gate,
    expert_gate,
    expert_up,
    expert_down,
    chosen,
    route_weight,
    dense_gate,
    dense_up,
    dense_down,
):
    smem = pl.BlockSpec(memory_space=pltpu.SMEM)
    vmem = pl.BlockSpec(memory_space=pltpu.VMEM)
    hbm = pl.BlockSpec(memory_space=ANY)
    dma = pltpu.SemaphoreType.DMA
    regular = pltpu.SemaphoreType.REGULAR
    scratch = [
        pltpu.VMEM((TOK, 1024, 128), BF16),
        pltpu.VMEM((TOK, 4, 1024), F32),
        pltpu.VMEM((2048, 256), BF16),
        pltpu.VMEM((128, 2048), BF16),
        pltpu.VMEM((4, 2048), BF16),
        pltpu.VMEM((256, 2048), BF16),
        pltpu.VMEM((2048, 256), BF16),
        pltpu.VMEM((2048, 256), BF16),
        pltpu.VMEM((256, 2048), BF16),
        pltpu.VMEM((2048, 256), BF16),
        pltpu.VMEM((2048, 256), BF16),
        pltpu.VMEM((256, 2048), BF16),
        pltpu.VMEM((NTP, TOK, W), BF16),
        pltpu.VMEM((64, 1024), F32),
        pltpu.VMEM((64, 256), F32),
        pltpu.VMEM((64, 1024), F32),
        pltpu.VMEM((64, 256), F32),
        pltpu.VMEM((NTP, TOK, W), BF16),
        pltpu.VMEM((NTP, TOK, W), BF16),
        pltpu.VMEM((512, 64), BF16),
        pltpu.VMEM((128, 512), BF16),
        pltpu.VMEM((512, 512), BF16),
        pltpu.VMEM((512, 512), BF16),
        pltpu.VMEM((TOK, W), BF16),
        pltpu.VMEM((NTP, TOK, W), BF16),
        pltpu.VMEM((NEP, 8, 128), BF16),
        pltpu.VMEM((NTP, NEP, 8, 128), BF16),
        pltpu.VMEM((128, 2048), BF16),
        pltpu.VMEM((NTP, TOK, W), BF16),
        pltpu.VMEM((NTP, TOK, W), BF16),
        pltpu.VMEM((NTP, 128, W), BF16),
        pltpu.VMEM((NTP, 128, W), BF16),
        pltpu.VMEM((NEP, 8, 128), BF16),
        pltpu.VMEM((NEP, 8, 128), BF16),
        pltpu.VMEM((16, 128), F32),
        dma((12,)),
        dma((8,)),
        dma,
        dma((NTP,)),
        regular,
        regular,
        dma,
        dma((NTP,)),
        dma,
        dma((NTP,)),
        dma,
        dma((NZ,)),
        dma,
        dma((NTP,)),
        dma,
        dma((NTP,)),
        dma,
        dma((NTP,)),
        dma,
        dma,
    ]
    return pl.pallas_call(
        layer,
        out_shape=jax.ShapeDtypeStruct((TOK, W), BF16),
        in_specs=[vmem, smem, smem, vmem, vmem, vmem, vmem, vmem] + [hbm] * 13,
        out_specs=vmem,
        scratch_shapes=scratch,
        compiler_params=pltpu.CompilerParams(collective_id=0, has_side_effects=True),
        name="layer",
    )(
        tokens,
        lengths,
        forget_bias,
        attn_gain.reshape(16, 128),
        ffn_gain.reshape(16, 128),
        mix_gate.reshape(16, 128),
        chosen.T,
        route_weight.T,
        kv_cache,
        cum_gate,
        w_query,
        w_key.T,
        w_value.T,
        w_forget.T,
        w_out,
        expert_gate[0],
        expert_up[0],
        expert_down[0],
        dense_gate,
        dense_up,
        dense_down,
    )


def solution(mesh):
    in_specs = (
        P("ep", "tp"),
        P("ep", None, "tp"),
        P("ep", "tp", None),
        P("ep"),
        P(None, "tp"),
        P(None, "tp"),
        P(None, "tp"),
        P(None, "tp"),
        P("tp"),
        P("tp", None),
        P(),
        P(),
        P(),
        P("ep", None, "tp"),
        P("ep", None, "tp"),
        P("ep", "tp", None),
        P("ep", None),
        P("ep", None),
        P(None, "tp"),
        P(None, "tp"),
        P("tp", None),
    )
    out_specs = P("ep", "tp")
    return jax.shard_map(local, mesh=mesh, in_specs=in_specs, out_specs=out_specs, check_vma=False)
```

time: 112 us -> 54.9 us (0.49)
  Pallas kernels: 0 us -> 53.4 us
  waiting for transfers between devices: 42.2 us -> 0 us
  starting transfers between devices: 37.5 us -> 0 us
  matrix products: 12.3 us -> 0 us
  local copies, waits for them, and re-layouts: 13.6 us -> 1.32 us
  other arithmetic: 5.45 us -> 0 us
    pallas_call x0 -> x1, Pallas kernels: none -> 53.4 us  [local(): pl.pallas_call(layer, out_shape=jax.ShapeDtypeStruct((TOK, W), BF16), in_...]
    all_to_all x6 -> x0, waiting for transfers between devices: 42.2 us -> none  [the longest x1 17.7 us: local(): lax.all_to_all(outgoing, 'ep', split_axis=0, concat_axis=0, tiled=True)]
    all_to_all x6 -> x0, starting transfers between devices: 37.5 us -> none  [the longest x1 14.3 us: local(): lax.all_to_all(outgoing, 'ep', split_axis=0, concat_axis=0, tiled=True)]
    dot_general x15 -> x0, matrix products: 12.3 us -> none  [the longest x1 2.31 us: local(): jnp.dot(dense_act, dense_down, preferred_element_type=jnp.float32)]
    unnamed x27 -> x1, local copies, waits for them, and re-layouts: 7.34 us -> 1.32 us
    reshape x8 -> x0, local copies, waits for them, and re-layouts: 3.75 us -> none  [the longest x2 1.48 us: in_blocks(): return jnp.moveaxis(array.reshape(*before, devices, -1, *after), dim, 0)]
    broadcast_in_dim x2 -> x0, local copies, waits for them, and re-layouts: 2.16 us -> none  [copy_for_each(): copies = jnp.broadcast_to(array, (lax.axis_size(axis), *array.shape))]
    convert_element_type x7 -> x0, other arithmetic: 1.62 us -> none  [the longest x1 0.73 us: local(): (residual.astype(jnp.float32) + routed_sum + blend_gate[:, None] * dense_...]
  transfers between devices with their start and end apart: 6 -> 0, of which waited for: 5 -> 0; matrix products, arithmetic and copies ran while one was open for 14% -> 0% of each run, Pallas kernels for 0% -> 0%
where the time goes in v1:
time: 54.9 us; the launch traced here: 54.7 us
  Pallas kernels  53.4 us (97%)
  local copies, waits for them, and re-layouts  1.32 us (2%)
    pallas_call x1, Pallas kernels, local(): pl.pallas_call(layer, out_shape=jax.ShapeDtypeStruct((TOK, W), BF16), in_...  53.4 us
    unnamed x1, local copies, waits for them, and re-layouts  1.32 us

profile of v1, /device:TPU:1, one launch (start us, length us, event | category | flops | bytes accessed | tf_op | source)
XLA Modules:
  0.0 54.7 jit_solution(13819862738097927804)
XLA Ops:
  0.0 53.4 %layer.1 = bf16[16,512]{1,0:T(8,128)(2,1)} custom-call(bf16[16,512]{1,0:T(8,128)(2,1)} %tokens.1, s32[16]{0:T(128)} %lengths.1, f32[4]{0:T(128)} %forget_bias.1, bf16[16,128]{1,0:T(8,128)(2,1)} %bitcast.17, bf16[16,128]{1,0:T(8,128)(2,1)} %bitcast.18, bf16[16,128]{1,0:T(8,128)(2,1)} %bitcast.19, s32[2,16]{1,0:T(2,128)} %bitcast.20, f32[2,16]{1,0:T(2,128)} %bitcast.21, ...), custom_call_target="tpu_custom_call" | custom-call | tf_op jit(solution)/shard_map/layer/pallas_call | solution.py:556
  53.4 1.3 %copy.23 = bf16[16,512]{1,0:T(8,128)(2,1)} copy(bf16[16,512]{1,0:T(8,128)(2,1)} %layer.1) | data formatting | bytes 32768

commit v2 on v1

--- a/solution.py
+++ b/solution.py
@@ -55,14 +55,14 @@
 
 
 def layer(
-    tokens,
-    lengths,
-    forget_bias,
-    attn_gain,
-    ffn_gain,
-    mix_gate,
-    chosen,
-    route_weight,
+    tokens_hbm,
+    lengths_hbm,
+    bias_hbm,
+    attn_hbm,
+    ffn_hbm,
+    mix_hbm,
+    chosen_hbm,
+    route_hbm,
     kv_hbm,
     cum_hbm,
     wq_hbm,
@@ -77,7 +77,16 @@
     du_hbm,
     dd_hbm,
     out,
+    tokens,
+    lengths,
+    forget_bias,
+    attn_gain,
+    ffn_gain,
+    mix_gate,
+    chosen,
+    route_weight,
     kv,
+    keys,
     cum,
     wq,
     wkv,
@@ -91,7 +100,6 @@
     dd,
     xbuf,
     gate,
-    q2,
     sc,
     ob,
     pbuf,
@@ -136,8 +144,11 @@
     ep = lax.axis_index("ep")
     tp = lax.axis_index("tp")
     z = ep // NR
-    r = ep % NR
-    peers = [(tp + i) % NTP for i in (2, 1, 3)]
+    r = lax.rem(ep, NR)
+    peers = [lax.rem(tp + i, NTP) for i in (2, 1, 3)]
+    planes = [lax.rem(z + i, NZ) for i in range(NZ)]
+    mates = [lax.rem(r + i, NR) for i in range(NR)]
+    order = (0, 1, 7, 2, 6, 3, 5, 4)
 
     def load(src, dst, i):
         copy = pltpu.make_async_copy(src, dst, load_sem.at[i])
@@ -165,26 +176,34 @@
         pl.semaphore_signal(barrier, inc=1, device_id={"tp": p}, device_id_type=MESH)
     for i in range(1, NR):
         pl.semaphore_signal(
-            barrier, inc=1, device_id={"ep": z * NR + (r + i) % NR}, device_id_type=MESH
+            barrier, inc=1, device_id={"ep": z * NR + mates[i]}, device_id_type=MESH
         )
     for i in (1, 2, 6, 7):
         pl.semaphore_signal(
-            barrier, inc=1, device_id={"ep": ((z + i) % NZ) * NR + r}, device_id_type=MESH
+            barrier, inc=1, device_id={"ep": planes[i] * NR + r}, device_id_type=MESH
         )
 
     loads = {}
+    loads["tokens"] = load(tokens_hbm, tokens, 12)
+    loads["lengths"] = load(lengths_hbm, lengths, 13)
     loads["cum"] = load(cum_hbm, cum, 0)
+    loads["chosen"] = load(chosen_hbm, chosen, 14)
+    loads["route"] = load(route_hbm, route_weight, 15)
+    loads["attn"] = load(attn_hbm, attn_gain, 16)
+    loads["ffn"] = load(ffn_hbm, ffn_gain, 17)
+    loads["mix"] = load(mix_hbm, mix_gate, 18)
+    loads["bias"] = load(bias_hbm, forget_bias, 19)
+
+    def kv_load(q):
+        part = pl.ds(4 * q, 4)
+        return pltpu.make_async_copy(kv_hbm.at[part], kv.at[part], kv_sem.at[q])
+
+    for q in range(4):
+        kv_load(q).start()
     loads["wk"] = load(wk_hbm, wkv.at[pl.ds(0, 64)], 1)
     loads["wv"] = load(wv_hbm, wkv.at[pl.ds(64, 64)], 2)
     loads["wf"] = load(wf_hbm, wf, 3)
     loads["wq"] = load(wq_hbm, wq, 4)
-    kv_loads = []
-    for p in range(8):
-        copy = pltpu.make_async_copy(
-            kv_hbm.at[pl.ds(2 * p, 2)], kv.at[pl.ds(2 * p, 2)], kv_sem.at[p]
-        )
-        copy.start()
-        kv_loads.append(copy)
     loads["wo"] = load(wo_hbm, wo, 5)
     loads["dg"] = load(dg_hbm, dg, 6)
     loads["du"] = load(du_hbm, du, 7)
@@ -193,18 +212,19 @@
     loads["eu"] = load(eu_hbm, eu, 10)
     loads["ed"] = load(ed_hbm, ed, 11)
 
+    loads["tokens"].wait()
     pl.semaphore_wait(barrier, 14)
 
     for p in peers:
         remote(tokens, xbuf.at[tp], x_send, x_recv.at[tp], {"tp": p}).start()
     for i in (2, 6):
         pl.semaphore_signal(
-            ready_a, inc=1, device_id={"ep": ((z + i) % NZ) * NR + r}, device_id_type=MESH
+            ready_a, inc=1, device_id={"ep": planes[i] * NR + r}, device_id_type=MESH
         )
     xbuf[tp] = tokens[...]
-    ffn32[...] = ffn_gain[...].astype(F32)
-
-    loads["cum"].wait()
+
+    for name in ("lengths", "cum"):
+        loads[name].wait()
 
     def gate_pair(p, carry):
         both = jnp.concatenate([cum[2 * p], cum[2 * p + 1]], axis=0)
@@ -219,12 +239,8 @@
 
     lax.fori_loop(0, 8, gate_pair, 0)
 
-    pl.semaphore_wait(ready_a, 2)
-    for i in range(1, NR):
-        pl.semaphore_signal(
-            ready_b, inc=1, device_id={"ep": z * NR + (r + i) % NR}, device_id_type=MESH
-        )
-
+    for name in ("chosen", "route"):
+        loads[name].wait()
     pick = chosen[...]
     expert = iota((NEP, TOK), 0)
     hot = [jnp.where(expert == pick[k : k + 1, :], 1.0, 0.0) for k in range(2)]
@@ -261,16 +277,23 @@
         for k in range(2)
     ]
 
-    def perm_part(i, carry):
-        base = pl.multiple_of(64 * i, 64)
-        a = iota((64, 512), 0) + base
-        b = iota((64, 512), 1)
-        perm[pl.ds(base, 64), :] = one_hot((a % 128) * 4 + a // 128 == b)
-        permt[pl.ds(base, 64), :] = one_hot((b % 128) * 4 + b // 128 == a)
+    def key_part(q, carry):
+        kv_load(q).wait()
+        for i in range(4):
+            turned = jnp.transpose(kv[4 * q + i])
+            keys[q, 64 * i : 64 * i + 64, :] = turned[0:64]
         return carry
 
-    lax.fori_loop(0, 8, perm_part, 0)
-
+    lax.fori_loop(0, 4, key_part, 0)
+
+    pl.semaphore_wait(ready_a, 2)
+    for i in range(1, NR):
+        pl.semaphore_signal(
+            ready_b, inc=1, device_id={"ep": z * NR + mates[i]}, device_id_type=MESH
+        )
+
+    for name in ("attn", "bias"):
+        loads[name].wait()
     for p in peers:
         arrived(xbuf.at[p], x_recv.at[p])
     x_full = jnp.concatenate([xbuf[p] for p in range(NTP)], axis=1).astype(F32)
@@ -310,13 +333,12 @@
     scale = HD ** (-0.5)
     own = jnp.sum(q64 * kv64, axis=1, keepdims=True) * scale - f64
     first = iota((64, 128), 0) % 8 < 4
-    q2[:, 0:128] = jnp.where(first, q64, 0.0)
-    q2[:, 128:256] = jnp.where(first, 0.0, q64)
-
-    for p in range(8):
-        kv_loads[p].wait()
-        keys = jnp.concatenate([kv[2 * p], kv[2 * p + 1]], axis=1)
-        sc[pl.ds(8 * p, 8), :] = dot_nt(q2[pl.ds(8 * p, 8), :].astype(BF16), keys)
+    wide = jnp.concatenate([q64, q64], axis=1)
+    wide = wide + pltpu.roll(wide, HD, 1)
+    own_lanes = (iota((64, 256), 0) // 4) % 4 == iota((64, 256), 1) // HD
+    blocks = jnp.where(own_lanes, wide, 0.0).astype(BF16)
+    for q in range(4):
+        sc[pl.ds(16 * q, 16), :] = dot(blocks[16 * q : 16 * q + 16], keys[q])
     score = sc[...] * scale + gate[...]
     highest = jnp.maximum(jnp.max(score, axis=1, keepdims=True), own)
     prob = jnp.exp(score - highest)
@@ -350,6 +372,19 @@
         remote(pbuf.at[p], abuf.at[tp], p_send, p_recv.at[tp], {"tp": p}).start()
     abuf[tp] = pbuf[tp]
 
+    def perm_part(i, carry):
+        base = pl.multiple_of(64 * i, 64)
+        a = iota((64, 512), 0) + base
+        b = iota((64, 512), 1)
+        perm[pl.ds(base, 64), :] = one_hot((a % 128) * 4 + a // 128 == b)
+        permt[pl.ds(base, 64), :] = one_hot((b % 128) * 4 + b // 128 == a)
+        return carry
+
+    lax.fori_loop(0, 8, perm_part, 0)
+
+    for name in ("ffn", "mix"):
+        loads[name].wait()
+    ffn32[...] = ffn_gain[...].astype(F32)
     pl.semaphore_wait(ready_b, 7)
 
     for p in peers:
@@ -363,22 +398,18 @@
     outgoing = dot(dmat[...], stacked)
     outg[...] = outgoing.reshape(NEP, 8, 128).astype(BF16)
 
-    def send_out(i, carry):
-        k = i // NR
-        dz = jnp.where(k % 2 == 1, 4 - (k + 1) // 2, (4 + k // 2) % 8)
-        dr = (r + i + 1) % NR
-        e = ((z + dz) % NZ) * NR + dr
-        remote(outg.at[e], gath.at[tp, ep], o_send, o_recv.at[z], {"ep": e}).start()
-        return carry
-
-    lax.fori_loop(0, 63, send_out, 0)
+    for dz in order:
+        for i in range(1, NR + 1):
+            if dz or i < NR:
+                e = planes[dz] * NR + mates[i % NR]
+                remote(outg.at[e], gath.at[tp, ep], o_send, o_recv.at[z], {"ep": e}).start()
     gath[tp, ep] = outg[ep]
     for p in peers:
         remote(resb, rbuf.at[tp], r_send, r_recv.at[tp], {"tp": p}).start()
     rbuf[tp] = resb[...]
 
-    for dz in (0, 1, 7, 2, 6, 3, 5, 4):
-        src_z = (z + dz) % NZ
+    for dz in order:
+        src_z = planes[dz]
         base = src_z * NR
         count = NR - 1 if dz == 0 else NR
         arrived(gath.at[tp, pl.ds(base, count)], o_recv.at[src_z])
@@ -408,7 +439,7 @@
         loads[name].wait()
     squares = jnp.zeros((128, 128), F32)
     for i in (0, 1, 3, 2):
-        p = (tp + i) % NTP
+        p = lax.rem(tp + i, NTP)
         if i:
             arrived(gath.at[p], g_recv.at[p])
         rows = dot(perm[...], gath[p].reshape(512, 128))
@@ -434,15 +465,11 @@
     stacked = jnp.concatenate([summed[:, f * 128 : (f + 1) * 128] for f in range(4)], axis=0)
     rout[...] = dot(permt[...], stacked).reshape(NEP, 8, 128).astype(BF16)
 
-    def send_back(i, carry):
-        k = i // NR
-        dz = jnp.where(k % 2 == 1, 4 - (k + 1) // 2, (4 + k // 2) % 8)
-        dr = (r + i + 1) % NR
-        e = ((z + dz) % NZ) * NR + dr
-        remote(rout.at[e], rin.at[ep], b_send, b_recv, {"ep": e}).start()
-        return carry
-
-    lax.fori_loop(0, 63, send_back, 0)
+    for dz in (4, 3, 5, 2, 6, 1, 7, 0):
+        for i in range(1, NR + 1):
+            if dz or i < NR:
+                e = planes[dz] * NR + mates[i % NR]
+                remote(rout.at[e], rin.at[ep], b_send, b_recv, {"ep": e}).start()
     rin[ep] = rout[ep]
 
     for p in peers:
@@ -491,13 +518,21 @@
     dense_up,
     dense_down,
 ):
-    smem = pl.BlockSpec(memory_space=pltpu.SMEM)
     vmem = pl.BlockSpec(memory_space=pltpu.VMEM)
     hbm = pl.BlockSpec(memory_space=ANY)
     dma = pltpu.SemaphoreType.DMA
     regular = pltpu.SemaphoreType.REGULAR
     scratch = [
+        pltpu.VMEM((TOK, W), BF16),
+        pltpu.SMEM((TOK,), jnp.int32),
+        pltpu.SMEM((4,), F32),
+        pltpu.VMEM((16, 128), BF16),
+        pltpu.VMEM((16, 128), BF16),
+        pltpu.VMEM((16, 128), BF16),
+        pltpu.VMEM((2, TOK), jnp.int32),
+        pltpu.VMEM((2, TOK), F32),
         pltpu.VMEM((TOK, 1024, 128), BF16),
+        pltpu.VMEM((4, 256, 1024), BF16),
         pltpu.VMEM((TOK, 4, 1024), F32),
         pltpu.VMEM((2048, 256), BF16),
         pltpu.VMEM((128, 2048), BF16),
@@ -511,7 +546,6 @@
         pltpu.VMEM((256, 2048), BF16),
         pltpu.VMEM((NTP, TOK, W), BF16),
         pltpu.VMEM((64, 1024), F32),
-        pltpu.VMEM((64, 256), F32),
         pltpu.VMEM((64, 1024), F32),
         pltpu.VMEM((64, 256), F32),
         pltpu.VMEM((NTP, TOK, W), BF16),
@@ -532,8 +566,8 @@
         pltpu.VMEM((NEP, 8, 128), BF16),
         pltpu.VMEM((NEP, 8, 128), BF16),
         pltpu.VMEM((16, 128), F32),
-        dma((12,)),
-        dma((8,)),
+        dma((20,)),
+        dma((4,)),
         dma,
         dma((NTP,)),
         regular,
@@ -555,8 +589,8 @@
     ]
     return pl.pallas_call(
         layer,
-        out_shape=jax.ShapeDtypeStruct((TOK, W), BF16),
-        in_specs=[vmem, smem, smem, vmem, vmem, vmem, vmem, vmem] + [hbm] * 13,
+        out_shape=pltpu.VMEM((TOK, W), BF16),
+        in_specs=[hbm] * 21,
         out_specs=vmem,
         scratch_shapes=scratch,
         compiler_params=pltpu.CompilerParams(collective_id=0, has_side_effects=True),

time: 54.9 us -> 48.8 us (0.89)
  Pallas kernels: 53.4 us -> 48 us
  local copies, waits for them, and re-layouts: 1.32 us -> 0.61 us
    pallas_call x1, Pallas kernels: 53.4 us -> 48 us  [local(): pl.pallas_call(layer, out_shape=pltpu.VMEM((TOK, W), BF16), in_specs=[hbm...]
    unnamed x1, local copies, waits for them, and re-layouts: 1.32 us -> 0.61 us
where the time goes in v2:
time: 48.8 us; the launch traced here: 48.7 us
  Pallas kernels  48 us (98%)
  local copies, waits for them, and re-layouts  0.61 us (1%)
    pallas_call x1, Pallas kernels, local(): pl.pallas_call(layer, out_shape=pltpu.VMEM((TOK, W), BF16), in_specs=[hbm...  48 us

profile of v2, /device:TPU:1, one launch (start us, length us, event | category | flops | bytes accessed | tf_op | source)
XLA Modules:
  0.0 48.7 jit_solution(197256472453400372)
XLA Ops:
  0.0 48.0 %layer.1 = bf16[16,512]{1,0:T(8,128)(2,1)S(1)} custom-call(bf16[16,512]{1,0:T(8,128)(2,1)} %tokens_hbm.1, s32[16]{0:T(128)} %lengths_hbm.1, f32[4]{0:T(128)} %bias_hbm.1, bf16[16,128]{1,0:T(8,128)(2,1)} %bitcast.17, bf16[16,128]{1,0:T(8,128)(2,1)} %bitcast.18, bf16[16,128]{1,0:T(8,128)(2,1)} %bitcast.19, s32[2,16]{1,0:T(2,128)} %bitcast.20, ...), custom_call_target="tpu_custom_call" | custom-call | tf_op jit(solution)/shard_map/layer/pallas_call | solution.py:590
  48.1 0.6 %copy.23 = bf16[16,512]{1,0:T(8,128)(2,1)} copy(bf16[16,512]{1,0:T(8,128)(2,1)S(1)} %layer.1) | data formatting | bytes 32768

commit v3 on v2

--- a/solution.py
+++ b/solution.py
@@ -18,6 +18,12 @@
 NR = 8
 NEP = 64
 W = 512
+NEAR = 3
+SN = NEAR * NR
+SF = NEP - SN
+SB = 16
+SA = SF - SB
+ORDER = (0, 1, 7, 2, 6, 3, 5, 4)
 NT = (((1,), (1,)), ((), ()))
 
 
@@ -87,6 +93,7 @@
     route_weight,
     kv,
     keys,
+    values,
     cum,
     wq,
     wkv,
@@ -105,20 +112,27 @@
     pbuf,
     abuf,
     dmat,
-    rmat,
-    perm,
-    permt,
+    rmat_n,
+    rmat_f,
+    perm_n,
+    permt_n,
+    perm_b,
+    permt_b,
     resb,
     rbuf,
     outg,
+    outn,
     gath,
     hbuf,
+    dpart,
     dsend,
     dbuf,
     ysend,
     ybuf,
     rout,
+    routn,
     rin,
+    rinn,
     ffn32,
     load_sem,
     kv_sem,
@@ -140,6 +154,9 @@
     y_recv,
     b_send,
     b_recv,
+    n_send,
+    c_send,
+    c_recv,
 ):
     ep = lax.axis_index("ep")
     tp = lax.axis_index("tp")
@@ -148,7 +165,6 @@
     peers = [lax.rem(tp + i, NTP) for i in (2, 1, 3)]
     planes = [lax.rem(z + i, NZ) for i in range(NZ)]
     mates = [lax.rem(r + i, NR) for i in range(NR)]
-    order = (0, 1, 7, 2, 6, 3, 5, 4)
 
     def load(src, dst, i):
         copy = pltpu.make_async_copy(src, dst, load_sem.at[i])
@@ -171,6 +187,8 @@
     def left(ref, sem):
         remote(ref, ref, sem, x_recv.at[0], {"tp": peers[0]}).wait_send()
 
+    loads = {}
+    loads["tokens"] = load(tokens_hbm, tokens, 12)
     barrier = pltpu.get_barrier_semaphore()
     for p in peers:
         pl.semaphore_signal(barrier, inc=1, device_id={"tp": p}, device_id_type=MESH)
@@ -183,8 +201,6 @@
             barrier, inc=1, device_id={"ep": planes[i] * NR + r}, device_id_type=MESH
         )
 
-    loads = {}
-    loads["tokens"] = load(tokens_hbm, tokens, 12)
     loads["lengths"] = load(lengths_hbm, lengths, 13)
     loads["cum"] = load(cum_hbm, cum, 0)
     loads["chosen"] = load(chosen_hbm, chosen, 14)
@@ -204,6 +220,16 @@
     loads["wv"] = load(wv_hbm, wkv.at[pl.ds(64, 64)], 2)
     loads["wf"] = load(wf_hbm, wf, 3)
     loads["wq"] = load(wq_hbm, wq, 4)
+    loads["tokens"].wait()
+    pl.semaphore_wait(barrier, 14)
+
+    for p in peers:
+        remote(tokens, xbuf.at[tp], x_send, x_recv.at[tp], {"tp": p}).start()
+    for i in (2, 6):
+        pl.semaphore_signal(
+            ready_a, inc=1, device_id={"ep": planes[i] * NR + r}, device_id_type=MESH
+        )
+    xbuf[tp] = tokens[...]
     loads["wo"] = load(wo_hbm, wo, 5)
     loads["dg"] = load(dg_hbm, dg, 6)
     loads["du"] = load(du_hbm, du, 7)
@@ -211,17 +237,6 @@
     loads["eg"] = load(eg_hbm, eg, 9)
     loads["eu"] = load(eu_hbm, eu, 10)
     loads["ed"] = load(ed_hbm, ed, 11)
-
-    loads["tokens"].wait()
-    pl.semaphore_wait(barrier, 14)
-
-    for p in peers:
-        remote(tokens, xbuf.at[tp], x_send, x_recv.at[tp], {"tp": p}).start()
-    for i in (2, 6):
-        pl.semaphore_signal(
-            ready_a, inc=1, device_id={"ep": planes[i] * NR + r}, device_id_type=MESH
-        )
-    xbuf[tp] = tokens[...]
 
     for name in ("lengths", "cum"):
         loads[name].wait()
@@ -239,49 +254,16 @@
 
     lax.fori_loop(0, 8, gate_pair, 0)
 
-    for name in ("chosen", "route"):
-        loads[name].wait()
-    pick = chosen[...]
-    expert = iota((NEP, TOK), 0)
-    hot = [jnp.where(expert == pick[k : k + 1, :], 1.0, 0.0) for k in range(2)]
-    earlier = one_hot(iota((TOK, TOK), 0) < iota((TOK, TOK), 1))
-    before = dot((hot[0] + hot[1]).astype(BF16), earlier)
-    slots = [
-        2.0 * pick[k : k + 1, :].astype(F32) + jnp.sum(hot[k] * before, axis=0, keepdims=True)
-        for k in range(2)
-    ]
-    weight = route_weight[...]
-    w_rows = [three_parts(weight[k : k + 1, :]) for k in range(2)]
-    info = jnp.concatenate(
-        slots + [part.astype(F32) for k in range(2) for part in w_rows[k]], axis=0
-    ).astype(BF16)
-    spread = one_hot(iota((TOK, 64), 0) == iota((TOK, 64), 1) % TOK)
-    spread_t = one_hot(iota((64, TOK), 0) % TOK == iota((64, TOK), 1))
-    info_rows = dot(info, spread).astype(jnp.int32)
-    info_cols = dot_nt(spread_t, info)
-    row = iota((512, 64), 0)
-    col_fb = iota((512, 64), 1) // TOK
-    dmask = jnp.zeros((512, 64), F32)
-    for k in range(2):
-        dmask = dmask + jnp.where(row == info_rows[k : k + 1, :] * 4 + col_fb, 1.0, 0.0)
-    dmat[...] = dmask.astype(BF16)
-    lane = iota((64, 512), 1)
-    row_fb = iota((64, 512), 0) // TOK
-    for k in range(2):
-        slot_col = info_cols[:, k : k + 1].astype(jnp.int32)
-        rmat[pl.ds(64 * k, 64), :] = one_hot(lane == slot_col * 4 + row_fb)
-    w_cols = [
-        info_cols[:, 2 + 3 * k : 3 + 3 * k]
-        + info_cols[:, 3 + 3 * k : 4 + 3 * k]
-        + info_cols[:, 4 + 3 * k : 5 + 3 * k]
-        for k in range(2)
-    ]
-
     def key_part(q, carry):
         kv_load(q).wait()
         for i in range(4):
             turned = jnp.transpose(kv[4 * q + i])
             keys[q, 64 * i : 64 * i + 64, :] = turned[0:64]
+        for i in range(2):
+            s = 4 * q + 2 * i
+            values[q, :, 128 * i : 128 * i + 128] = jnp.concatenate(
+                [kv[s][:, HD:128], kv[s + 1][:, HD:128]], axis=1
+            )
         return carry
 
     lax.fori_loop(0, 4, key_part, 0)
@@ -332,7 +314,6 @@
     )
     scale = HD ** (-0.5)
     own = jnp.sum(q64 * kv64, axis=1, keepdims=True) * scale - f64
-    first = iota((64, 128), 0) % 8 < 4
     wide = jnp.concatenate([q64, q64], axis=1)
     wide = wide + pltpu.roll(wide, HD, 1)
     own_lanes = (iota((64, 256), 0) // 4) % 4 == iota((64, 256), 1) // HD
@@ -347,10 +328,11 @@
     inverse = 1.0 / total
     sc[...] = prob * inverse
     own_prob = own_prob * inverse
-    for p in range(8):
-        values = jnp.concatenate([kv[2 * p], kv[2 * p + 1]], axis=1)
-        ob[pl.ds(8 * p, 8), :] = dot(sc[pl.ds(8 * p, 8), :].astype(BF16), values)
-    blended = jnp.where(first, ob[:, 0:128], ob[:, 128:256])
+    for q in range(4):
+        ob[pl.ds(16 * q, 16), :] = dot(sc[pl.ds(16 * q, 16), :].astype(BF16), values[q])
+    seq = (iota((64, 128), 0) // 4) % 4
+    blended = jnp.where(seq < 2, ob[:, 0:128], ob[:, 128:256])
+    blended = jnp.where(seq % 2 == 0, pltpu.roll(blended, HD, 1), blended)
     blended = (blended + own_prob.astype(BF16).astype(F32) * kv64).astype(BF16)
     back = one_hot(
         iota((64, 64), 1) == (iota((64, 64), 0) % TOK) * 4 + iota((64, 64), 0) // TOK
@@ -372,15 +354,59 @@
         remote(pbuf.at[p], abuf.at[tp], p_send, p_recv.at[tp], {"tp": p}).start()
     abuf[tp] = pbuf[tp]
 
-    def perm_part(i, carry):
-        base = pl.multiple_of(64 * i, 64)
-        a = iota((64, 512), 0) + base
-        b = iota((64, 512), 1)
-        perm[pl.ds(base, 64), :] = one_hot((a % 128) * 4 + a // 128 == b)
-        permt[pl.ds(base, 64), :] = one_hot((b % 128) * 4 + b // 128 == a)
-        return carry
-
-    lax.fori_loop(0, 8, perm_part, 0)
+    for name in ("chosen", "route"):
+        loads[name].wait()
+    pick = chosen[...]
+    expert = iota((NEP, TOK), 0)
+    hot = [jnp.where(expert == pick[k : k + 1, :], 1.0, 0.0) for k in range(2)]
+    earlier = one_hot(iota((TOK, TOK), 0) < iota((TOK, TOK), 1))
+    before = dot((hot[0] + hot[1]).astype(BF16), earlier)
+    away = lax.rem(pick // NR - z + NZ, NZ)
+    order = jnp.where(away <= 4, jnp.maximum(2 * away - 1, 0), 16 - 2 * away)
+    place = 2.0 * (order * NR + lax.rem(pick, NR)).astype(F32)
+    slots = [
+        place[k : k + 1, :] + jnp.sum(hot[k] * before, axis=0, keepdims=True)
+        for k in range(2)
+    ]
+    weight = route_weight[...]
+    w_rows = [three_parts(weight[k : k + 1, :]) for k in range(2)]
+    info = jnp.concatenate(
+        slots + [part.astype(F32) for k in range(2) for part in w_rows[k]], axis=0
+    ).astype(BF16)
+    spread = one_hot(iota((TOK, 64), 0) == iota((TOK, 64), 1) % TOK)
+    spread_t = one_hot(iota((64, TOK), 0) % TOK == iota((64, TOK), 1))
+    info_rows = dot(info, spread).astype(jnp.int32)
+    info_cols = dot_nt(spread_t, info)
+    row = iota((512, 64), 0)
+    col_fb = iota((512, 64), 1) // TOK
+    dmask = jnp.zeros((512, 64), F32)
+    for k in range(2):
+        dmask = dmask + jnp.where(row == info_rows[k : k + 1, :] * 4 + col_fb, 1.0, 0.0)
+    dmat[...] = dmask.astype(BF16)
+    for k in range(2):
+        slot_col = info_cols[:, k : k + 1].astype(jnp.int32) * 4
+        for ref, lo, n in ((rmat_n, 0, 8 * SN), (rmat_f, 8 * SN, 8 * SF)):
+            lane = iota((64, n), 1) + lo
+            row_fb = iota((64, n), 0) // TOK
+            ref[pl.ds(64 * k, 64), :] = one_hot(lane == slot_col + row_fb)
+    w_cols = [
+        info_cols[:, 2 + 3 * k : 3 + 3 * k]
+        + info_cols[:, 3 + 3 * k : 4 + 3 * k]
+        + info_cols[:, 4 + 3 * k : 5 + 3 * k]
+        for k in range(2)
+    ]
+
+    for n, ref, ref_t in ((SN, perm_n, permt_n), (SB, perm_b, permt_b)):
+
+        def perm_part(i, carry, n=n, ref=ref, ref_t=ref_t):
+            base = pl.multiple_of(64 * i, 64)
+            a = iota((64, 8 * n), 0) + base
+            b = iota((64, 8 * n), 1)
+            ref[pl.ds(base, 64), :] = one_hot(lax.rem(a, 2 * n) * 4 + a // (2 * n) == b)
+            ref_t[pl.ds(base, 64), :] = one_hot(lax.rem(b, 2 * n) * 4 + b // (2 * n) == a)
+            return carry
+
+        lax.fori_loop(0, n // 8, perm_part, 0)
 
     for name in ("ffn", "mix"):
         loads[name].wait()
@@ -394,31 +420,61 @@
         attention = attention + abuf[p].astype(F32)
     residual = (tokens[...].astype(F32) + attention).astype(BF16)
     resb[...] = residual
-    stacked = jnp.concatenate([residual[:, f * 128 : (f + 1) * 128] for f in range(4)], axis=0)
-    outgoing = dot(dmat[...], stacked)
-    outg[...] = outgoing.reshape(NEP, 8, 128).astype(BF16)
-
-    for dz in order:
+    for p in peers:
+        remote(resb, rbuf.at[tp], r_send, r_recv.at[tp], {"tp": p}).start()
+    rbuf[tp] = residual
+
+    def stack(rows):
+        return jnp.concatenate([rows[:, f * 128 : (f + 1) * 128] for f in range(4)], axis=0)
+
+    def unstack(rows):
+        return jnp.concatenate([rows[16 * f : 16 * f + 16] for f in range(4)], axis=1)
+
+    def block(b):
+        return ORDER.index((NZ - ORDER[b]) % NZ)
+
+    def mine(b):
+        return block(b) * NR + r
+
+    outgoing = dot(dmat[pl.ds(8 * SN, 8 * SF), :], stack(residual))
+    outg[...] = outgoing.reshape(SF, 8, 128).astype(BF16)
+    for b in range(NEAR, NZ):
+        dz = ORDER[b]
         for i in range(1, NR + 1):
-            if dz or i < NR:
-                e = planes[dz] * NR + mates[i % NR]
-                remote(outg.at[e], gath.at[tp, ep], o_send, o_recv.at[z], {"ep": e}).start()
-    gath[tp, ep] = outg[ep]
-    for p in peers:
-        remote(resb, rbuf.at[tp], r_send, r_recv.at[tp], {"tp": p}).start()
-    rbuf[tp] = resb[...]
-
-    for dz in order:
-        src_z = planes[dz]
-        base = src_z * NR
-        count = NR - 1 if dz == 0 else NR
-        arrived(gath.at[tp, pl.ds(base, count)], o_recv.at[src_z])
-        chunk = gath.at[tp, pl.ds(base, NR)]
+            m = mates[i % NR]
+            remote(
+                outg.at[(b - NEAR) * NR + m],
+                gath.at[tp, mine(b)],
+                o_send,
+                o_recv.at[block(b)],
+                {"ep": planes[dz] * NR + m},
+            ).start()
+    for p in peers:
+        arrived(rbuf.at[p], r_recv.at[p])
+    for q in range(NTP):
+        outgoing = dot(dmat[pl.ds(0, 8 * SN), :], stack(rbuf[q]))
+        outn[:, q] = outgoing.reshape(SN, 8, 128).astype(BF16)
+    for b in range(NEAR):
+        dz = ORDER[b]
+        for i in range(1, NR + 1):
+            if b or i < NR:
+                m = mates[i % NR]
+                remote(
+                    outn.at[b * NR + m],
+                    gath.at[:, mine(b)],
+                    n_send,
+                    o_recv.at[block(b)],
+                    {"ep": planes[dz] * NR + m},
+                ).start()
+    gath[:, r] = outn[r]
+
+    for b in range(NEAR, NZ):
+        chunk = gath.at[tp, pl.ds(b * NR, NR)]
+        arrived(chunk, o_recv.at[b])
         for p in peers:
-            remote(chunk, chunk, g_send, g_recv.at[tp], {"tp": p}).start()
-
-    for p in peers:
-        arrived(rbuf.at[p], r_recv.at[p])
+            half = 0 if b < NEAR + 2 else 1
+            remote(chunk, chunk, g_send, g_recv.at[half, tp], {"tp": p}).start()
+
     res_full = jnp.concatenate([rbuf[p] for p in range(NTP)], axis=1).astype(F32)
     square = jnp.mean(res_full * res_full, axis=1, keepdims=True)
     ffn_row = gain_row(ffn_gain)
@@ -426,73 +482,129 @@
     for name in ("dg", "du", "dd"):
         loads[name].wait()
     dense_act = (silu(dot(h_two, dg[...])) * dot(h_two, du[...])).astype(BF16)
-    dense_part = dot(dense_act, dd[...]).astype(BF16)
-    for p in range(NTP):
-        dsend[p] = dense_part[:, p * W : (p + 1) * W]
-    for p in peers:
-        remote(dsend.at[p], dbuf.at[tp], d_send, d_recv.at[tp], {"tp": p}).start()
-    dbuf[tp] = dsend[tp]
     mixing = jnp.sum(h_two.astype(F32) * gain_row(mix_gate), axis=1, keepdims=True)
     blend = 1.0 / (1.0 + jnp.exp(-mixing))
-
+    dpart[...] = dot(dense_act, dd[...]) * blend
     for name in ("eg", "eu", "ed"):
         loads[name].wait()
-    squares = jnp.zeros((128, 128), F32)
-    for i in (0, 1, 3, 2):
-        p = lax.rem(tp + i, NTP)
-        if i:
-            arrived(gath.at[p], g_recv.at[p])
-        rows = dot(perm[...], gath[p].reshape(512, 128))
-        for f in range(4):
-            block = rows[128 * f : 128 * f + 128]
-            squares = squares + block * block
-            c = p * 4 + f
-            scaled = block * ffn32[pl.ds(c, 1), :]
-            hbuf[:, pl.ds(pl.multiple_of(c * 128, 128), 128)] = scaled.astype(BF16)
-    root = lax.rsqrt(jnp.sum(squares, axis=1, keepdims=True) * (1.0 / 2048.0) + EPS)
+
+    def expert_hidden(lo, n, perm, sources):
+        squares = jnp.zeros((2 * n, 128), F32)
+        for p, sem in sources:
+            if sem is not None:
+                arrived(gath.at[p, pl.ds(lo, n)], sem)
+            rows = dot(perm[...], gath[p, pl.ds(lo, n)].reshape(8 * n, 128))
+            for f in range(4):
+                part = rows[2 * n * f : 2 * n * (f + 1)]
+                squares = squares + part * part
+                c = p * 4 + f
+                scaled = part * ffn32[pl.ds(c, 1), :]
+                start = c * 128 if isinstance(c, int) else pl.multiple_of(c * 128, 128)
+                hbuf[2 * lo : 2 * (lo + n), pl.ds(start, 128)] = scaled.astype(BF16)
+        return lax.rsqrt(jnp.sum(squares, axis=1, keepdims=True) * (1.0 / 2048.0) + EPS)
+
+    for b in range(NEAR):
+        lo = 0 if b else 1
+        arrived(gath.at[:, pl.ds(b * NR + lo, NR - lo)], o_recv.at[b])
+    root_n = expert_hidden(0, SN, perm_n, [(p, None) for p in range(NTP)])
+    others = [lax.rem(tp + i, NTP) for i in (1, 3, 2)]
+    root_b = expert_hidden(
+        SN, SB, perm_b, [(tp, None)] + [(p, g_recv.at[0, p]) for p in others]
+    )
+    root_a = expert_hidden(
+        SN + SB, SA, perm_n, [(tp, None)] + [(p, g_recv.at[1, p]) for p in others]
+    )
+    root = jnp.concatenate([root_n, root_b, root_a], axis=0)
     hidden = hbuf[...]
     gate_pre = dot(hidden, eg[...]) * root
     up_pre = dot(hidden, eu[...]) * root
     act = (silu(gate_pre) * up_pre).astype(BF16)
-    for p in peers:
-        ysend[p] = dot(act, ed[:, pl.ds(pl.multiple_of(p * W, W), W)]).astype(BF16)
-        remote(ysend.at[p], ybuf.at[tp], y_send, y_recv.at[tp], {"tp": p}).start()
-    summed = dot(act, ed[:, pl.ds(pl.multiple_of(tp * W, W), W)]).astype(BF16).astype(F32)
-    for p in peers:
-        arrived(ybuf.at[p], y_recv.at[p])
-        summed = summed + ybuf[p].astype(F32)
-    summed = summed.astype(BF16)
-    stacked = jnp.concatenate([summed[:, f * 128 : (f + 1) * 128] for f in range(4)], axis=0)
-    rout[...] = dot(permt[...], stacked).reshape(NEP, 8, 128).astype(BF16)
-
-    for dz in (4, 3, 5, 2, 6, 1, 7, 0):
+    act_f = act[2 * SN : 128]
+    for p in peers:
+        ysend[p] = dot(act_f, ed[:, pl.ds(pl.multiple_of(p * W, W), W)]).astype(BF16)
+        part = pl.ds(2 * SB, 2 * SA)
+        remote(
+            ysend.at[p, part], ybuf.at[tp, part], y_send, y_recv.at[1, tp], {"tp": p}
+        ).start()
+    for p in peers:
+        part = pl.ds(0, 2 * SB)
+        remote(
+            ysend.at[p, part], ybuf.at[tp, part], y_send, y_recv.at[0, tp], {"tp": p}
+        ).start()
+    act_n = act[0 : 2 * SN]
+    for q in range(NTP):
+        part = dot(act_n, ed[:, q * W : (q + 1) * W]).astype(BF16)
+        turned = dot(permt_n[...], stack(part))
+        routn[:, q] = turned.reshape(SN, 8, 128).astype(BF16)
+    for b in range(NEAR):
+        dz = ORDER[b]
         for i in range(1, NR + 1):
-            if dz or i < NR:
-                e = planes[dz] * NR + mates[i % NR]
-                remote(rout.at[e], rin.at[ep], b_send, b_recv, {"ep": e}).start()
-    rin[ep] = rout[ep]
-
+            if b or i < NR:
+                m = mates[i % NR]
+                remote(
+                    routn.at[b * NR + m],
+                    rinn.at[mine(b)],
+                    c_send,
+                    c_recv,
+                    {"ep": planes[dz] * NR + m},
+                ).start()
+    rinn[r] = routn[r]
+
+    summed = dot(act_f, ed[:, pl.ds(pl.multiple_of(tp * W, W), W)]).astype(BF16).astype(F32)
+    for half, lo, n, turn, first, last in (
+        (1, SB, SA, permt_n, NEAR + 2, NZ),
+        (0, 0, SB, permt_b, NEAR, NEAR + 2),
+    ):
+        rows = summed[2 * lo : 2 * (lo + n)]
+        for p in peers:
+            part = pl.ds(2 * lo, 2 * n)
+            arrived(ybuf.at[p, part], y_recv.at[half, p])
+            rows = rows + ybuf[p, part].astype(F32)
+        turned = dot(turn[...], stack(rows.astype(BF16)))
+        rout[pl.ds(lo, n)] = turned.reshape(n, 8, 128).astype(BF16)
+        for b in reversed(range(first, last)):
+            dz = ORDER[b]
+            for i in range(1, NR + 1):
+                m = mates[i % NR]
+                remote(
+                    rout.at[(b - NEAR) * NR + m],
+                    rin.at[mine(b) - SN],
+                    b_send,
+                    b_recv,
+                    {"ep": planes[dz] * NR + m},
+                ).start()
+
+    def routed(picked):
+        return unstack(picked[0:64] * w_cols[0] + picked[64:128] * w_cols[1])
+
+    arrived(rinn.at[pl.ds(0, SN - 1)], c_recv)
+    for i in (2, 1, 3, 0):
+        q = lax.rem(tp + i, NTP)
+        part = routed(dot(rmat_n[...], rinn[:, q].reshape(8 * SN, 128)))
+        part = part + dpart[:, pl.ds(pl.multiple_of(q * W, W), W)]
+        if i:
+            dsend[q] = part.astype(BF16)
+            remote(dsend.at[q], dbuf.at[tp], d_send, d_recv.at[tp], {"tp": q}).start()
+        else:
+            mixed = residual.astype(F32) + part
+
+    arrived(rin, b_recv)
+    mixed = mixed + routed(dot(rmat_f[...], rin[...].reshape(8 * SF, 128)))
     for p in peers:
         arrived(dbuf.at[p], d_recv.at[p])
-    dense_out = dbuf[0].astype(F32)
-    for p in range(1, NTP):
-        dense_out = dense_out + dbuf[p].astype(F32)
-    mixed = residual.astype(F32) + blend * dense_out
-
-    arrived(rin.at[pl.ds(0, 63)], b_recv)
-    picked = dot(rmat[...], rin[...].reshape(512, 128))
-    routed = picked[0:64] * w_cols[0] + picked[64:128] * w_cols[1]
-    routed = jnp.concatenate([routed[16 * f : 16 * f + 16] for f in range(4)], axis=1)
-    out[...] = (mixed + routed).astype(BF16)
+        mixed = mixed + dbuf[p].astype(F32)
+    out[...] = mixed.astype(BF16)
 
     left(xbuf.at[pl.ds(0, 3)], x_send)
     left(pbuf.at[pl.ds(0, 3)], p_send)
     left(rbuf.at[pl.ds(0, 3)], r_send)
-    left(outg.at[pl.ds(0, 63)], o_send)
-    left(gath.at[pl.ds(0, 3)], g_send)
+    left(outg, o_send)
+    left(outn.at[pl.ds(0, SN - 1)], n_send)
+    left(gath.at[pl.ds(0, 3), pl.ds(SN, SF)], g_send)
     left(dsend.at[pl.ds(0, 3)], d_send)
     left(ysend.at[pl.ds(0, 3)], y_send)
-    left(rout.at[pl.ds(0, 63)], b_send)
+    left(rout, b_send)
+    left(routn.at[pl.ds(0, SN - 1)], c_send)
 
 
 def local(
@@ -533,6 +645,7 @@
         pltpu.VMEM((2, TOK), F32),
         pltpu.VMEM((TOK, 1024, 128), BF16),
         pltpu.VMEM((4, 256, 1024), BF16),
+        pltpu.VMEM((4, 1024, 256), BF16),
         pltpu.VMEM((TOK, 4, 1024), F32),
         pltpu.VMEM((2048, 256), BF16),
         pltpu.VMEM((128, 2048), BF16),
@@ -551,20 +664,27 @@
         pltpu.VMEM((NTP, TOK, W), BF16),
         pltpu.VMEM((NTP, TOK, W), BF16),
         pltpu.VMEM((512, 64), BF16),
-        pltpu.VMEM((128, 512), BF16),
-        pltpu.VMEM((512, 512), BF16),
-        pltpu.VMEM((512, 512), BF16),
+        pltpu.VMEM((128, 8 * SN), BF16),
+        pltpu.VMEM((128, 8 * SF), BF16),
+        pltpu.VMEM((8 * SN, 8 * SN), BF16),
+        pltpu.VMEM((8 * SN, 8 * SN), BF16),
+        pltpu.VMEM((8 * SB, 8 * SB), BF16),
+        pltpu.VMEM((8 * SB, 8 * SB), BF16),
         pltpu.VMEM((TOK, W), BF16),
         pltpu.VMEM((NTP, TOK, W), BF16),
-        pltpu.VMEM((NEP, 8, 128), BF16),
+        pltpu.VMEM((SF, 8, 128), BF16),
+        pltpu.VMEM((SN, NTP, 8, 128), BF16),
         pltpu.VMEM((NTP, NEP, 8, 128), BF16),
         pltpu.VMEM((128, 2048), BF16),
+        pltpu.VMEM((TOK, 2048), F32),
         pltpu.VMEM((NTP, TOK, W), BF16),
         pltpu.VMEM((NTP, TOK, W), BF16),
-        pltpu.VMEM((NTP, 128, W), BF16),
-        pltpu.VMEM((NTP, 128, W), BF16),
-        pltpu.VMEM((NEP, 8, 128), BF16),
-        pltpu.VMEM((NEP, 8, 128), BF16),
+        pltpu.VMEM((NTP, 2 * SF, W), BF16),
+        pltpu.VMEM((NTP, 2 * SF, W), BF16),
+        pltpu.VMEM((SF, 8, 128), BF16),
+        pltpu.VMEM((SN, NTP, 8, 128), BF16),
+        pltpu.VMEM((SF, 8, 128), BF16),
+        pltpu.VMEM((SN, NTP, 8, 128), BF16),
         pltpu.VMEM((16, 128), F32),
         dma((20,)),
         dma((4,)),
@@ -579,11 +699,14 @@
         dma,
         dma((NZ,)),
         dma,
+        dma((2, NTP)),
+        dma,
         dma((NTP,)),
         dma,
-        dma((NTP,)),
-        dma,
-        dma((NTP,)),
+        dma((2, NTP)),
+        dma,
+        dma,
+        dma,
         dma,
         dma,
     ]

time: 48.8 us -> 43.2 us (0.89)
  Pallas kernels: 48 us -> 42.5 us
    pallas_call x1, Pallas kernels: 48 us -> 42.5 us  [local(): pl.pallas_call(layer, out_shape=pltpu.VMEM((TOK, W), BF16), in_specs=[hbm...]
where the time goes in v3:
time: 43.2 us; the launch traced here: 43.1 us
  Pallas kernels  42.5 us (98%)
  local copies, waits for them, and re-layouts  0.61 us (1%)
    pallas_call x1, Pallas kernels, local(): pl.pallas_call(layer, out_shape=pltpu.VMEM((TOK, W), BF16), in_specs=[hbm...  42.5 us

profile of v3, /device:TPU:1, one launch (start us, length us, event | category | flops | bytes accessed | tf_op | source)
XLA Modules:
  0.0 43.1 jit_solution(6460124001075133433)
XLA Ops:
  0.0 42.5 %layer.1 = bf16[16,512]{1,0:T(8,128)(2,1)S(1)} custom-call(bf16[16,512]{1,0:T(8,128)(2,1)} %tokens_hbm.1, s32[16]{0:T(128)} %lengths_hbm.1, f32[4]{0:T(128)} %bias_hbm.1, bf16[16,128]{1,0:T(8,128)(2,1)} %bitcast.17, bf16[16,128]{1,0:T(8,128)(2,1)} %bitcast.18, bf16[16,128]{1,0:T(8,128)(2,1)} %bitcast.19, s32[2,16]{1,0:T(2,128)} %bitcast.20, ...), custom_call_target="tpu_custom_call" | custom-call | tf_op jit(solution)/shard_map/layer/pallas_call | solution.py:713
  42.5 0.6 %copy.23 = bf16[16,512]{1,0:T(8,128)(2,1)} copy(bf16[16,512]{1,0:T(8,128)(2,1)S(1)} %layer.1) | data formatting | bytes 32768

commit v4 on v3

--- a/solution.py
+++ b/solution.py
@@ -19,6 +19,8 @@
 NEP = 64
 W = 512
 NEAR = 3
+DIRECT = 5
+SD = DIRECT * NR
 SN = NEAR * NR
 SF = NEP - SN
 SB = 16
@@ -118,7 +120,7 @@
     permt_n,
     perm_b,
     permt_b,
-    resb,
+    permt_c,
     rbuf,
     outg,
     outn,
@@ -134,6 +136,7 @@
     rin,
     rinn,
     ffn32,
+    attn32,
     load_sem,
     kv_sem,
     x_send,
@@ -142,7 +145,6 @@
     ready_b,
     p_send,
     p_recv,
-    r_send,
     r_recv,
     o_send,
     o_recv,
@@ -276,17 +278,32 @@
 
     for name in ("attn", "bias"):
         loads[name].wait()
-    for p in peers:
-        arrived(xbuf.at[p], x_recv.at[p])
-    x_full = jnp.concatenate([xbuf[p] for p in range(NTP)], axis=1).astype(F32)
-    square = jnp.mean(x_full * x_full, axis=1, keepdims=True)
-    h_one = (x_full * lax.rsqrt(square + EPS) * gain_row(attn_gain)).astype(BF16)
-
+    attn32[...] = attn_gain[...].astype(F32)
     for name in ("wk", "wv", "wf", "wq"):
         loads[name].wait()
-    query = dot(h_one, wq[...]).astype(BF16)
-    kv_new = dot_nt(h_one, wkv[...]).astype(BF16)
-    forget = dot_nt(h_one, wf[...])
+    squares = jnp.zeros((TOK, 128), F32)
+    query = jnp.zeros((TOK, 256), F32)
+    kv_new = jnp.zeros((TOK, 128), F32)
+    forget = jnp.zeros((TOK, 4), F32)
+    for i in (0, 1, 3, 2):
+        p = lax.rem(tp + i, NTP)
+        if i:
+            arrived(xbuf.at[p], x_recv.at[p])
+        rows = xbuf[p].astype(F32)
+        scaled = []
+        for f in range(4):
+            part = rows[:, 128 * f : 128 * f + 128]
+            squares = squares + part * part
+            scaled.append((part * attn32[pl.ds(4 * p + f, 1), :]).astype(BF16))
+        scaled = jnp.concatenate(scaled, axis=1)
+        span = pl.ds(pl.multiple_of(p * W, W), W)
+        query = query + dot(scaled, wq[span, :])
+        kv_new = kv_new + dot_nt(scaled, wkv[:, span])
+        forget = forget + dot_nt(scaled, wf[:, span])
+    root = lax.rsqrt(jnp.sum(squares, axis=1, keepdims=True) * (1.0 / 2048.0) + EPS)
+    query = (query * root).astype(BF16)
+    kv_new = (kv_new * root).astype(BF16)
+    forget = forget * root
     head_lane = iota((TOK, 4), 1)
     bias = jnp.zeros((TOK, 4), F32)
     for h in range(4):
@@ -326,14 +343,13 @@
     own_prob = jnp.exp(own - highest)
     total = jnp.sum(prob, axis=1, keepdims=True) + own_prob
     inverse = 1.0 / total
-    sc[...] = prob * inverse
-    own_prob = own_prob * inverse
+    sc[...] = prob
     for q in range(4):
         ob[pl.ds(16 * q, 16), :] = dot(sc[pl.ds(16 * q, 16), :].astype(BF16), values[q])
     seq = (iota((64, 128), 0) // 4) % 4
     blended = jnp.where(seq < 2, ob[:, 0:128], ob[:, 128:256])
     blended = jnp.where(seq % 2 == 0, pltpu.roll(blended, HD, 1), blended)
-    blended = (blended + own_prob.astype(BF16).astype(F32) * kv64).astype(BF16)
+    blended = ((blended + own_prob * kv64) * inverse).astype(BF16)
     back = one_hot(
         iota((64, 64), 1) == (iota((64, 64), 0) % TOK) * 4 + iota((64, 64), 0) // TOK
     )
@@ -347,12 +363,15 @@
         axis=1,
     ).astype(BF16)
     loads["wo"].wait()
-    partial = dot(head_out, wo[...]).astype(BF16)
-    for p in range(NTP):
-        pbuf[p] = partial[:, p * W : (p + 1) * W]
     for p in peers:
-        remote(pbuf.at[p], abuf.at[tp], p_send, p_recv.at[tp], {"tp": p}).start()
-    abuf[tp] = pbuf[tp]
+        pbuf[p] = dot(head_out, wo[:, pl.ds(pl.multiple_of(p * W, W), W)]).astype(BF16)
+        remote(pbuf.at[p], abuf.at[tp, p], p_send, p_recv.at[tp], {"tp": p}).start()
+    pbuf[tp] = dot(head_out, wo[:, pl.ds(pl.multiple_of(tp * W, W), W)]).astype(BF16)
+    for i in (1, 2, 3):
+        for p in peers:
+            q = lax.rem(p + i, NTP)
+            remote(pbuf.at[q], abuf.at[tp, q], p_send, r_recv.at[tp], {"tp": p}).start()
+    abuf[tp] = pbuf[...]
 
     for name in ("chosen", "route"):
         loads[name].wait()
@@ -396,17 +415,21 @@
         for k in range(2)
     ]
 
-    for n, ref, ref_t in ((SN, perm_n, permt_n), (SB, perm_b, permt_b)):
+    for n, ref, ref_t in ((SN, perm_n, permt_n), (SB, perm_b, permt_b), (NR, None, permt_c)):
 
         def perm_part(i, carry, n=n, ref=ref, ref_t=ref_t):
-            base = pl.multiple_of(64 * i, 64)
+            base = 0 if n == NR else pl.multiple_of(64 * i, 64)
             a = iota((64, 8 * n), 0) + base
             b = iota((64, 8 * n), 1)
-            ref[pl.ds(base, 64), :] = one_hot(lax.rem(a, 2 * n) * 4 + a // (2 * n) == b)
+            if ref is not None:
+                ref[pl.ds(base, 64), :] = one_hot(lax.rem(a, 2 * n) * 4 + a // (2 * n) == b)
             ref_t[pl.ds(base, 64), :] = one_hot(lax.rem(b, 2 * n) * 4 + b // (2 * n) == a)
             return carry
 
-        lax.fori_loop(0, n // 8, perm_part, 0)
+        if n > NR:
+            lax.fori_loop(0, n // NR, perm_part, 0)
+        else:
+            perm_part(0, 0)
 
     for name in ("ffn", "mix"):
         loads[name].wait()
@@ -414,15 +437,14 @@
     pl.semaphore_wait(ready_b, 7)
 
     for p in peers:
-        arrived(abuf.at[p], p_recv.at[p])
-    attention = abuf[0].astype(F32)
-    for p in range(1, NTP):
-        attention = attention + abuf[p].astype(F32)
-    residual = (tokens[...].astype(F32) + attention).astype(BF16)
-    resb[...] = residual
-    for p in peers:
-        remote(resb, rbuf.at[tp], r_send, r_recv.at[tp], {"tp": p}).start()
-    rbuf[tp] = residual
+        arrived(abuf.at[p, tp], p_recv.at[p])
+    def residual_of(q):
+        attention = abuf[0, q].astype(F32)
+        for p in range(1, NTP):
+            attention = attention + abuf[p, q].astype(F32)
+        return (xbuf[q].astype(F32) + attention).astype(BF16)
+
+    residual = residual_of(tp)
 
     def stack(rows):
         return jnp.concatenate([rows[:, f * 128 : (f + 1) * 128] for f in range(4)], axis=0)
@@ -436,25 +458,28 @@
     def mine(b):
         return block(b) * NR + r
 
-    outgoing = dot(dmat[pl.ds(8 * SN, 8 * SF), :], stack(residual))
-    outg[...] = outgoing.reshape(SF, 8, 128).astype(BF16)
-    for b in range(NEAR, NZ):
+    outgoing = dot(dmat[pl.ds(8 * SD, 8 * SA), :], stack(residual))
+    outg[...] = outgoing.reshape(SA, 8, 128).astype(BF16)
+    for b in range(DIRECT, NZ):
         dz = ORDER[b]
         for i in range(1, NR + 1):
             m = mates[i % NR]
             remote(
-                outg.at[(b - NEAR) * NR + m],
+                outg.at[(b - DIRECT) * NR + m],
                 gath.at[tp, mine(b)],
                 o_send,
                 o_recv.at[block(b)],
                 {"ep": planes[dz] * NR + m},
             ).start()
     for p in peers:
-        arrived(rbuf.at[p], r_recv.at[p])
+        arrived(abuf.at[p, pl.ds(0, 3)], r_recv.at[p])
     for q in range(NTP):
-        outgoing = dot(dmat[pl.ds(0, 8 * SN), :], stack(rbuf[q]))
-        outn[:, q] = outgoing.reshape(SN, 8, 128).astype(BF16)
-    for b in range(NEAR):
+        rbuf[q] = residual_of(q)
+    wide = jnp.concatenate([stack(rbuf[q]) for q in range(NTP)], axis=1)
+    outgoing = dot(dmat[pl.ds(0, 8 * SD), :], wide)
+    for q in range(NTP):
+        outn[:, q] = outgoing[:, 128 * q : 128 * q + 128].reshape(SD, 8, 128).astype(BF16)
+    for b in range(DIRECT):
         dz = ORDER[b]
         for i in range(1, NR + 1):
             if b or i < NR:
@@ -468,12 +493,11 @@
                 ).start()
     gath[:, r] = outn[r]
 
-    for b in range(NEAR, NZ):
+    for b in range(DIRECT, NZ):
         chunk = gath.at[tp, pl.ds(b * NR, NR)]
         arrived(chunk, o_recv.at[b])
         for p in peers:
-            half = 0 if b < NEAR + 2 else 1
-            remote(chunk, chunk, g_send, g_recv.at[half, tp], {"tp": p}).start()
+            remote(chunk, chunk, g_send, g_recv.at[tp], {"tp": p}).start()
 
     res_full = jnp.concatenate([rbuf[p] for p in range(NTP)], axis=1).astype(F32)
     square = jnp.mean(res_full * res_full, axis=1, keepdims=True)
@@ -488,54 +512,77 @@
     for name in ("eg", "eu", "ed"):
         loads[name].wait()
 
-    def expert_hidden(lo, n, perm, sources):
+    def scaled_rows(rows, lo, n, c):
+        start = c * 128 if isinstance(c, int) else pl.multiple_of(c * 128, 128)
+        hbuf[2 * lo : 2 * (lo + n), pl.ds(start, 128)] = (rows * ffn32[pl.ds(c, 1), :]).astype(
+            BF16
+        )
+        return rows * rows
+
+    def root_of(squares):
+        return lax.rsqrt(jnp.sum(squares, axis=1, keepdims=True) * (1.0 / 2048.0) + EPS)
+
+    def direct_rows(lo, n, perm):
+        wide = jnp.concatenate(
+            [gath[q, pl.ds(lo, n)].reshape(8 * n, 128) for q in range(NTP)], axis=1
+        )
+        rows = dot(perm[...], wide)
         squares = jnp.zeros((2 * n, 128), F32)
-        for p, sem in sources:
-            if sem is not None:
-                arrived(gath.at[p, pl.ds(lo, n)], sem)
-            rows = dot(perm[...], gath[p, pl.ds(lo, n)].reshape(8 * n, 128))
+        for q in range(NTP):
             for f in range(4):
-                part = rows[2 * n * f : 2 * n * (f + 1)]
-                squares = squares + part * part
-                c = p * 4 + f
-                scaled = part * ffn32[pl.ds(c, 1), :]
-                start = c * 128 if isinstance(c, int) else pl.multiple_of(c * 128, 128)
-                hbuf[2 * lo : 2 * (lo + n), pl.ds(start, 128)] = scaled.astype(BF16)
-        return lax.rsqrt(jnp.sum(squares, axis=1, keepdims=True) * (1.0 / 2048.0) + EPS)
-
-    for b in range(NEAR):
+                part = rows[2 * n * f : 2 * n * (f + 1), 128 * q : 128 * q + 128]
+                squares = squares + scaled_rows(part, lo, n, 4 * q + f)
+        return root_of(squares)
+
+    for b in range(DIRECT):
         lo = 0 if b else 1
         arrived(gath.at[:, pl.ds(b * NR + lo, NR - lo)], o_recv.at[b])
-    root_n = expert_hidden(0, SN, perm_n, [(p, None) for p in range(NTP)])
-    others = [lax.rem(tp + i, NTP) for i in (1, 3, 2)]
-    root_b = expert_hidden(
-        SN, SB, perm_b, [(tp, None)] + [(p, g_recv.at[0, p]) for p in others]
-    )
-    root_a = expert_hidden(
-        SN + SB, SA, perm_n, [(tp, None)] + [(p, g_recv.at[1, p]) for p in others]
-    )
-    root = jnp.concatenate([root_n, root_b, root_a], axis=0)
-    hidden = hbuf[...]
-    gate_pre = dot(hidden, eg[...]) * root
-    up_pre = dot(hidden, eu[...]) * root
-    act = (silu(gate_pre) * up_pre).astype(BF16)
-    act_f = act[2 * SN : 128]
+    root_n = direct_rows(0, SN, perm_n)
+    root_b = direct_rows(SN, SB, perm_b)
+    root = jnp.concatenate([root_n, root_b], axis=0)
+    hidden = hbuf[0 : 2 * SD]
+    act_d = silu(dot(hidden, eg[...]) * root) * (dot(hidden, eu[...]) * root)
+    act_d = act_d.astype(BF16)
+    act_b = act_d[2 * SN : 2 * SD]
+    part = pl.ds(0, 2 * SB)
     for p in peers:
-        ysend[p] = dot(act_f, ed[:, pl.ds(pl.multiple_of(p * W, W), W)]).astype(BF16)
-        part = pl.ds(2 * SB, 2 * SA)
-        remote(
-            ysend.at[p, part], ybuf.at[tp, part], y_send, y_recv.at[1, tp], {"tp": p}
-        ).start()
-    for p in peers:
-        part = pl.ds(0, 2 * SB)
+        ysend[p, part] = dot(act_b, ed[:, pl.ds(pl.multiple_of(p * W, W), W)]).astype(BF16)
         remote(
             ysend.at[p, part], ybuf.at[tp, part], y_send, y_recv.at[0, tp], {"tp": p}
         ).start()
-    act_n = act[0 : 2 * SN]
+    squares = jnp.zeros((2 * SA, 128), F32)
+    gate_pre = jnp.zeros((2 * SA, 256), F32)
+    up_pre = jnp.zeros((2 * SA, 256), F32)
+    for i in (0, 1, 3, 2):
+        p = lax.rem(tp + i, NTP)
+        if i:
+            arrived(gath.at[p, pl.ds(SD, SA)], g_recv.at[p])
+        rows = dot(perm_n[...], gath[p, pl.ds(SD, SA)].reshape(8 * SA, 128))
+        for f in range(4):
+            part = rows[2 * SA * f : 2 * SA * (f + 1)]
+            squares = squares + scaled_rows(part, SD, SA, 4 * p + f)
+        span = pl.ds(pl.multiple_of(p * W, W), W)
+        hidden = hbuf[2 * SD : 128, span]
+        gate_pre = gate_pre + dot(hidden, eg[span, :])
+        up_pre = up_pre + dot(hidden, eu[span, :])
+    root_a = root_of(squares)
+    act_f = (silu(gate_pre * root_a) * (up_pre * root_a)).astype(BF16)
+    for half, lo, n in ((2, 32, NR), (1, 16, SB)):
+        part = pl.ds(2 * lo, 2 * n)
+        for p in peers:
+            if half == 2:
+                ysend[p, pl.ds(2 * SB, 2 * SA)] = dot(
+                    act_f, ed[:, pl.ds(pl.multiple_of(p * W, W), W)]
+                ).astype(BF16)
+            remote(
+                ysend.at[p, part], ybuf.at[tp, part], y_send, y_recv.at[half, tp], {"tp": p}
+            ).start()
+    act_n = act_d[0 : 2 * SN]
+    part = dot(act_n, ed[...]).astype(BF16)
+    wide = jnp.concatenate([stack(part[:, q * W : (q + 1) * W]) for q in range(NTP)], axis=1)
+    turned = dot(permt_n[...], wide)
     for q in range(NTP):
-        part = dot(act_n, ed[:, q * W : (q + 1) * W]).astype(BF16)
-        turned = dot(permt_n[...], stack(part))
-        routn[:, q] = turned.reshape(SN, 8, 128).astype(BF16)
+        routn[:, q] = turned[:, 128 * q : 128 * q + 128].reshape(SN, 8, 128).astype(BF16)
     for b in range(NEAR):
         dz = ORDER[b]
         for i in range(1, NR + 1):
@@ -550,12 +597,14 @@
                 ).start()
     rinn[r] = routn[r]
 
-    summed = dot(act_f, ed[:, pl.ds(pl.multiple_of(tp * W, W), W)]).astype(BF16).astype(F32)
-    for half, lo, n, turn, first, last in (
-        (1, SB, SA, permt_n, NEAR + 2, NZ),
-        (0, 0, SB, permt_b, NEAR, NEAR + 2),
+    own_cols = ed[:, pl.ds(pl.multiple_of(tp * W, W), W)]
+    sum_b = dot(act_b, own_cols).astype(BF16).astype(F32)
+    sum_a = dot(act_f, own_cols).astype(BF16).astype(F32)
+    for half, lo, n, turn, first, last, rows in (
+        (0, 0, SB, permt_b, 3, 5, sum_b),
+        (2, 32, NR, permt_c, 7, 8, sum_a[32:48]),
+        (1, 16, SB, permt_b, 5, 7, sum_a[0:32]),
     ):
-        rows = summed[2 * lo : 2 * (lo + n)]
         for p in peers:
             part = pl.ds(2 * lo, 2 * n)
             arrived(ybuf.at[p, part], y_recv.at[half, p])
@@ -578,10 +627,14 @@
         return unstack(picked[0:64] * w_cols[0] + picked[64:128] * w_cols[1])
 
     arrived(rinn.at[pl.ds(0, SN - 1)], c_recv)
+    wide = jnp.concatenate([rinn[:, q].reshape(8 * SN, 128) for q in range(NTP)], axis=1)
+    picked = dot(rmat_n[...], wide)
+    for q in range(NTP):
+        part = routed(picked[:, 128 * q : 128 * q + 128])
+        dpart[:, q * W : (q + 1) * W] = part + dpart[:, q * W : (q + 1) * W]
     for i in (2, 1, 3, 0):
         q = lax.rem(tp + i, NTP)
-        part = routed(dot(rmat_n[...], rinn[:, q].reshape(8 * SN, 128)))
-        part = part + dpart[:, pl.ds(pl.multiple_of(q * W, W), W)]
+        part = dpart[:, pl.ds(pl.multiple_of(q * W, W), W)]
         if i:
             dsend[q] = part.astype(BF16)
             remote(dsend.at[q], dbuf.at[tp], d_send, d_recv.at[tp], {"tp": q}).start()
@@ -596,11 +649,10 @@
     out[...] = mixed.astype(BF16)
 
     left(xbuf.at[pl.ds(0, 3)], x_send)
-    left(pbuf.at[pl.ds(0, 3)], p_send)
-    left(rbuf.at[pl.ds(0, 3)], r_send)
+    left(abuf.at[pl.ds(0, 3)], p_send)
     left(outg, o_send)
-    left(outn.at[pl.ds(0, SN - 1)], n_send)
-    left(gath.at[pl.ds(0, 3), pl.ds(SN, SF)], g_send)
+    left(outn.at[pl.ds(0, SD - 1)], n_send)
+    left(gath.at[pl.ds(0, 3), pl.ds(SD, SA)], g_send)
     left(dsend.at[pl.ds(0, 3)], d_send)
     left(ysend.at[pl.ds(0, 3)], y_send)
     left(rout, b_send)
@@ -662,7 +714,7 @@
         pltpu.VMEM((64, 1024), F32),
         pltpu.VMEM((64, 256), F32),
         pltpu.VMEM((NTP, TOK, W), BF16),
-        pltpu.VMEM((NTP, TOK, W), BF16),
+        pltpu.VMEM((NTP, NTP, TOK, W), BF16),
         pltpu.VMEM((512, 64), BF16),
         pltpu.VMEM((128, 8 * SN), BF16),
         pltpu.VMEM((128, 8 * SF), BF16),
@@ -670,10 +722,10 @@
         pltpu.VMEM((8 * SN, 8 * SN), BF16),
         pltpu.VMEM((8 * SB, 8 * SB), BF16),
         pltpu.VMEM((8 * SB, 8 * SB), BF16),
-        pltpu.VMEM((TOK, W), BF16),
+        pltpu.VMEM((64, 64), BF16),
         pltpu.VMEM((NTP, TOK, W), BF16),
-        pltpu.VMEM((SF, 8, 128), BF16),
-        pltpu.VMEM((SN, NTP, 8, 128), BF16),
+        pltpu.VMEM((SA, 8, 128), BF16),
+        pltpu.VMEM((SD, NTP, 8, 128), BF16),
         pltpu.VMEM((NTP, NEP, 8, 128), BF16),
         pltpu.VMEM((128, 2048), BF16),
         pltpu.VMEM((TOK, 2048), F32),
@@ -686,6 +738,7 @@
         pltpu.VMEM((SF, 8, 128), BF16),
         pltpu.VMEM((SN, NTP, 8, 128), BF16),
         pltpu.VMEM((16, 128), F32),
+        pltpu.VMEM((16, 128), F32),
         dma((20,)),
         dma((4,)),
         dma,
@@ -694,16 +747,15 @@
         regular,
         dma,
         dma((NTP,)),
-        dma,
         dma((NTP,)),
         dma,
         dma((NZ,)),
         dma,
-        dma((2, NTP)),
-        dma,
         dma((NTP,)),
         dma,
-        dma((2, NTP)),
+        dma((NTP,)),
+        dma,
+        dma((3, NTP)),
         dma,
         dma,
         dma,

time: 43.2 us -> 41.5 us (0.961)
  Pallas kernels: 42.5 us -> 40.7 us
    pallas_call x1, Pallas kernels: 42.5 us -> 40.7 us  [local(): pl.pallas_call(layer, out_shape=pltpu.VMEM((TOK, W), BF16), in_specs=[hbm...]
where the time goes in v4:
time: 41.5 us; the launch traced here: 41.4 us
  Pallas kernels  40.7 us (98%)
  local copies, waits for them, and re-layouts  0.61 us (1%)
    pallas_call x1, Pallas kernels, local(): pl.pallas_call(layer, out_shape=pltpu.VMEM((TOK, W), BF16), in_specs=[hbm...  40.7 us

profile of v4, /device:TPU:1, one launch (start us, length us, event | category | flops | bytes accessed | tf_op | source)
XLA Modules:
  0.0 41.4 jit_solution(1312987952936673800)
XLA Ops:
  0.0 40.7 %layer.1 = bf16[16,512]{1,0:T(8,128)(2,1)S(1)} custom-call(bf16[16,512]{1,0:T(8,128)(2,1)} %tokens_hbm.1, s32[16]{0:T(128)} %lengths_hbm.1, f32[4]{0:T(128)} %bias_hbm.1, bf16[16,128]{1,0:T(8,128)(2,1)} %bitcast.17, bf16[16,128]{1,0:T(8,128)(2,1)} %bitcast.18, bf16[16,128]{1,0:T(8,128)(2,1)} %bitcast.19, s32[2,16]{1,0:T(2,128)} %bitcast.20, ...), custom_call_target="tpu_custom_call" | custom-call | tf_op jit(solution)/shard_map/layer/pallas_call | solution.py:765
  40.8 0.6 %copy.23 = bf16[16,512]{1,0:T(8,128)(2,1)} copy(bf16[16,512]{1,0:T(8,128)(2,1)S(1)} %layer.1) | data formatting | bytes 32768

commit v5 on v4

--- a/solution.py
+++ b/solution.py
@@ -109,8 +109,6 @@
     dd,
     xbuf,
     gate,
-    sc,
-    ob,
     pbuf,
     abuf,
     dmat,
@@ -243,18 +241,17 @@
     for name in ("lengths", "cum"):
         loads[name].wait()
 
-    def gate_pair(p, carry):
-        both = jnp.concatenate([cum[2 * p], cum[2 * p + 1]], axis=0)
-        row = iota((8, 1024), 0)
-        pos = iota((8, 1024), 1)
-        length = jnp.where(row < 4, lengths[2 * p], lengths[2 * p + 1])
-        last = jnp.sum(jnp.where(pos == length - 1, both, 0.0), axis=1, keepdims=True)
-        gate[pl.ds(pl.multiple_of(8 * p, 8), 8), :] = jnp.where(
-            pos < length, last - both, -jnp.inf
-        )
-        return carry
-
-    lax.fori_loop(0, 8, gate_pair, 0)
+    seq_row = iota((TOK, 1), 0)
+    length = jnp.zeros((TOK, 1), jnp.int32)
+    for i in range(TOK):
+        length = jnp.where(seq_row == i, lengths[i], length)
+    pos = iota((TOK, 1024), 1)
+    for h in range(4):
+        rows = cum[:, h, :]
+        last = jnp.sum(jnp.where(pos == length - 1, rows, 0.0), axis=1, keepdims=True)
+        rows = jnp.where(pos < length, last - rows, -jnp.inf)
+        for q in range(4):
+            gate[16 * q + 4 * h : 16 * q + 4 * h + 4, :] = rows[4 * q : 4 * q + 4]
 
     def key_part(q, carry):
         kv_load(q).wait()
@@ -311,54 +308,52 @@
     forget = forget + bias
     forget = jnp.minimum(forget, 0.0) - jnp.log1p(jnp.exp(-jnp.abs(forget)))
 
-    row64 = iota((64, TOK), 0)
-    col16 = iota((64, TOK), 1)
-    repeat = one_hot(row64 // 4 == col16)
-    row32 = iota((64, 32), 0)
-    col32 = iota((64, 32), 1)
-    even = one_hot((row32 // 4 == col32 % TOK) & (row32 % 4 == (col32 // TOK) * 2))
-    odd = one_hot((row32 // 4 == col32 % TOK) & (row32 % 4 == (col32 // TOK) * 2 + 1))
-    stacked = jnp.concatenate([query[:, 0:128], query[:, 128:256]], axis=0)
-    low_half = iota((64, 128), 1) < HD
-    q64 = jnp.where(
-        low_half, dot(even, stacked) + pltpu.roll(dot(odd, stacked), HD, 1), 0.0
+    low = iota((TOK, 128), 1) < HD
+    heads = []
+    for pair in (query[:, 0:128], query[:, 128:256]):
+        pair = pair.astype(F32)
+        other = pltpu.roll(pair, HD, 1)
+        heads += [jnp.where(low, pair, other), jnp.where(low, other, pair)]
+    def by_quad(per_head):
+        return jnp.concatenate(
+            [per_head[h][4 * q : 4 * q + 4] for q in range(4) for h in range(4)], axis=0
+        )
+
+    heads = by_quad(heads)
+    kv64 = by_quad([kv_new.astype(F32)] * 4)
+    f64 = by_quad([forget[:, h : h + 1] for h in range(4)])
+    low64 = iota((64, 128), 1) < HD
+    scale = HD ** (-0.5)
+    own = jnp.sum(jnp.where(low64, heads * kv64, 0.0), axis=1, keepdims=True) * scale - f64
+    mine_only = iota((64, 256), 1) // HD == iota((64, 256), 0) % 4
+    blocks = jnp.where(mine_only, jnp.concatenate([heads] * 2, axis=1), 0.0).astype(BF16)
+    score = jnp.concatenate(
+        [dot(blocks[16 * q : 16 * q + 16], keys[q]) for q in range(4)], axis=0
     )
-    kv64 = dot(repeat, kv_new)
-    f_parts = three_parts(forget)
-    f64 = dot(repeat, f_parts[0]) + dot(repeat, f_parts[1]) + dot(repeat, f_parts[2])
-    f64 = jnp.sum(
-        jnp.where(iota((64, 4), 0) % 4 == iota((64, 4), 1), f64, 0.0), axis=1, keepdims=True
-    )
-    scale = HD ** (-0.5)
-    own = jnp.sum(q64 * kv64, axis=1, keepdims=True) * scale - f64
-    wide = jnp.concatenate([q64, q64], axis=1)
-    wide = wide + pltpu.roll(wide, HD, 1)
-    own_lanes = (iota((64, 256), 0) // 4) % 4 == iota((64, 256), 1) // HD
-    blocks = jnp.where(own_lanes, wide, 0.0).astype(BF16)
-    for q in range(4):
-        sc[pl.ds(16 * q, 16), :] = dot(blocks[16 * q : 16 * q + 16], keys[q])
-    score = sc[...] * scale + gate[...]
+    score = score * scale + gate[...]
     highest = jnp.maximum(jnp.max(score, axis=1, keepdims=True), own)
     prob = jnp.exp(score - highest)
     own_prob = jnp.exp(own - highest)
-    total = jnp.sum(prob, axis=1, keepdims=True) + own_prob
-    inverse = 1.0 / total
-    sc[...] = prob
-    for q in range(4):
-        ob[pl.ds(16 * q, 16), :] = dot(sc[pl.ds(16 * q, 16), :].astype(BF16), values[q])
-    seq = (iota((64, 128), 0) // 4) % 4
-    blended = jnp.where(seq < 2, ob[:, 0:128], ob[:, 128:256])
-    blended = jnp.where(seq % 2 == 0, pltpu.roll(blended, HD, 1), blended)
-    blended = ((blended + own_prob * kv64) * inverse).astype(BF16)
-    back = one_hot(
-        iota((64, 64), 1) == (iota((64, 64), 0) % TOK) * 4 + iota((64, 64), 0) // TOK
+    inverse = 1.0 / (jnp.sum(prob, axis=1, keepdims=True) + own_prob)
+    prob = prob.astype(BF16)
+    mixed_values = jnp.concatenate(
+        [dot(prob[16 * q : 16 * q + 16], values[q]) for q in range(4)], axis=0
     )
-    heads = dot(back, blended)
-    low16 = iota((TOK, 128), 1) < HD
+    mixed_values = jnp.where(mine_only, mixed_values, 0.0)
+    blended = mixed_values[:, 0:128] + mixed_values[:, 128:256]
+    blended = blended + pltpu.roll(blended, HD, 1)
+    value_row = jnp.where(low64, pltpu.roll(kv64, HD, 1), kv64)
+    blended = (blended + own_prob * value_row) * inverse
+    per_head = [
+        jnp.concatenate(
+            [blended[16 * q + 4 * h : 16 * q + 4 * h + 4] for q in range(4)], axis=0
+        )
+        for h in range(4)
+    ]
     head_out = jnp.concatenate(
         [
-            jnp.where(low16, pltpu.roll(heads[0:16], HD, 1), heads[16:32]),
-            jnp.where(low16, pltpu.roll(heads[32:48], HD, 1), heads[48:64]),
+            jnp.where(low, per_head[0], per_head[1]),
+            jnp.where(low, per_head[2], per_head[3]),
         ],
         axis=1,
     ).astype(BF16)
@@ -534,6 +529,26 @@
                 squares = squares + scaled_rows(part, lo, n, 4 * q + f)
         return root_of(squares)
 
+    def far_source(sources):
+        wide = jnp.concatenate(
+            [gath[p, pl.ds(SD, SA)].reshape(8 * SA, 128) for p in sources], axis=1
+        )
+        rows = dot(perm_n[...], wide)
+        squares = jnp.zeros((2 * SA, 128), F32)
+        gate_pre = jnp.zeros((2 * SA, 256), F32)
+        up_pre = jnp.zeros((2 * SA, 256), F32)
+        for k, p in enumerate(sources):
+            for f in range(4):
+                part = rows[2 * SA * f : 2 * SA * (f + 1), 128 * k : 128 * k + 128]
+                squares = squares + scaled_rows(part, SD, SA, 4 * p + f)
+        for p in sources:
+            span = pl.ds(pl.multiple_of(p * W, W), W)
+            hidden = hbuf[2 * SD : 128, span]
+            gate_pre = gate_pre + dot(hidden, eg[span, :])
+            up_pre = up_pre + dot(hidden, eu[span, :])
+        return squares, gate_pre, up_pre
+
+    far = far_source([tp])
     for b in range(DIRECT):
         lo = 0 if b else 1
         arrived(gath.at[:, pl.ds(b * NR + lo, NR - lo)], o_recv.at[b])
@@ -550,21 +565,12 @@
         remote(
             ysend.at[p, part], ybuf.at[tp, part], y_send, y_recv.at[0, tp], {"tp": p}
         ).start()
-    squares = jnp.zeros((2 * SA, 128), F32)
-    gate_pre = jnp.zeros((2 * SA, 256), F32)
-    up_pre = jnp.zeros((2 * SA, 256), F32)
-    for i in (0, 1, 3, 2):
-        p = lax.rem(tp + i, NTP)
-        if i:
-            arrived(gath.at[p, pl.ds(SD, SA)], g_recv.at[p])
-        rows = dot(perm_n[...], gath[p, pl.ds(SD, SA)].reshape(8 * SA, 128))
-        for f in range(4):
-            part = rows[2 * SA * f : 2 * SA * (f + 1)]
-            squares = squares + scaled_rows(part, SD, SA, 4 * p + f)
-        span = pl.ds(pl.multiple_of(p * W, W), W)
-        hidden = hbuf[2 * SD : 128, span]
-        gate_pre = gate_pre + dot(hidden, eg[span, :])
-        up_pre = up_pre + dot(hidden, eu[span, :])
+    sides = [lax.rem(tp + 1, NTP), lax.rem(tp + 3, NTP)]
+    for p in sides:
+        arrived(gath.at[p, pl.ds(SD, SA)], g_recv.at[p])
+    far = [a + b for a, b in zip(far, far_source(sides))]
+    arrived(gath.at[peers[0], pl.ds(SD, SA)], g_recv.at[peers[0]])
+    squares, gate_pre, up_pre = [a + b for a, b in zip(far, far_source(peers[:1]))]
     root_a = root_of(squares)
     act_f = (silu(gate_pre * root_a) * (up_pre * root_a)).astype(BF16)
     for half, lo, n in ((2, 32, NR), (1, 16, SB)):
@@ -711,8 +717,6 @@
         pltpu.VMEM((256, 2048), BF16),
         pltpu.VMEM((NTP, TOK, W), BF16),
         pltpu.VMEM((64, 1024), F32),
-        pltpu.VMEM((64, 1024), F32),
-        pltpu.VMEM((64, 256), F32),
         pltpu.VMEM((NTP, TOK, W), BF16),
         pltpu.VMEM((NTP, NTP, TOK, W), BF16),
         pltpu.VMEM((512, 64), BF16),

time: 41.5 us -> 41.2 us (level)
  no operation moved by 1% of the time
where the time goes in v5:
time: 41.2 us; the launch traced here: 41 us
  Pallas kernels  40.4 us (98%)
  local copies, waits for them, and re-layouts  0.61 us (1%)
    pallas_call x1, Pallas kernels, local(): pl.pallas_call(layer, out_shape=pltpu.VMEM((TOK, W), BF16), in_specs=[hbm...  40.4 us

profile of v5, /device:TPU:1, one launch (start us, length us, event | category | flops | bytes accessed | tf_op | source)
XLA Modules:
  0.0 41.0 jit_solution(12265483866268835882)
XLA Ops:
  0.0 40.4 %layer.1 = bf16[16,512]{1,0:T(8,128)(2,1)S(1)} custom-call(bf16[16,512]{1,0:T(8,128)(2,1)} %tokens_hbm.1, s32[16]{0:T(128)} %lengths_hbm.1, f32[4]{0:T(128)} %bias_hbm.1, bf16[16,128]{1,0:T(8,128)(2,1)} %bitcast.17, bf16[16,128]{1,0:T(8,128)(2,1)} %bitcast.18, bf16[16,128]{1,0:T(8,128)(2,1)} %bitcast.19, s32[2,16]{1,0:T(2,128)} %bitcast.20, ...), custom_call_target="tpu_custom_call" | custom-call | tf_op jit(solution)/shard_map/layer/pallas_call | solution.py:769
  40.4 0.6 %copy.23 = bf16[16,512]{1,0:T(8,128)(2,1)} copy(bf16[16,512]{1,0:T(8,128)(2,1)S(1)} %layer.1) | data formatting | bytes 32768

commit v6 on v5

--- a/solution.py
+++ b/solution.py
@@ -113,6 +113,7 @@
     abuf,
     dmat,
     rmat_n,
+    rmat_b,
     rmat_f,
     perm_n,
     permt_n,
@@ -399,7 +400,11 @@
     dmat[...] = dmask.astype(BF16)
     for k in range(2):
         slot_col = info_cols[:, k : k + 1].astype(jnp.int32) * 4
-        for ref, lo, n in ((rmat_n, 0, 8 * SN), (rmat_f, 8 * SN, 8 * SF)):
+        for ref, lo, n in (
+            (rmat_n, 0, 8 * SN),
+            (rmat_b, 8 * SN, 8 * SB),
+            (rmat_f, 8 * SD, 8 * SA),
+        ):
             lane = iota((64, n), 1) + lo
             row_fb = iota((64, n), 0) // TOK
             ref[pl.ds(64 * k, 64), :] = one_hot(lane == slot_col + row_fb)
@@ -625,7 +630,7 @@
                     rout.at[(b - NEAR) * NR + m],
                     rin.at[mine(b) - SN],
                     b_send,
-                    b_recv,
+                    b_recv.at[min(half, 1)],
                     {"ep": planes[dz] * NR + m},
                 ).start()
 
@@ -647,11 +652,13 @@
         else:
             mixed = residual.astype(F32) + part
 
-    arrived(rin, b_recv)
-    mixed = mixed + routed(dot(rmat_f[...], rin[...].reshape(8 * SF, 128)))
+    arrived(rin.at[pl.ds(0, SB)], b_recv.at[0])
+    mixed = mixed + routed(dot(rmat_b[...], rin[pl.ds(0, SB)].reshape(8 * SB, 128)))
     for p in peers:
         arrived(dbuf.at[p], d_recv.at[p])
         mixed = mixed + dbuf[p].astype(F32)
+    arrived(rin.at[pl.ds(SB, SA)], b_recv.at[1])
+    mixed = mixed + routed(dot(rmat_f[...], rin[pl.ds(SB, SA)].reshape(8 * SA, 128)))
     out[...] = mixed.astype(BF16)
 
     left(xbuf.at[pl.ds(0, 3)], x_send)
@@ -721,7 +728,8 @@
         pltpu.VMEM((NTP, NTP, TOK, W), BF16),
         pltpu.VMEM((512, 64), BF16),
         pltpu.VMEM((128, 8 * SN), BF16),
-        pltpu.VMEM((128, 8 * SF), BF16),
+        pltpu.VMEM((128, 8 * SB), BF16),
+        pltpu.VMEM((128, 8 * SA), BF16),
         pltpu.VMEM((8 * SN, 8 * SN), BF16),
         pltpu.VMEM((8 * SN, 8 * SN), BF16),
         pltpu.VMEM((8 * SB, 8 * SB), BF16),
@@ -761,7 +769,7 @@
         dma,
         dma((3, NTP)),
         dma,
-        dma,
+        dma((2,)),
         dma,
         dma,
         dma,

time: 41.2 us -> 41.1 us (level)
  no operation moved by 1% of the time
where the time goes in v6:
time: 41.1 us; the launch traced here: 40.9 us
  Pallas kernels  40.3 us (98%)
  local copies, waits for them, and re-layouts  0.61 us (1%)
    pallas_call x1, Pallas kernels, local(): pl.pallas_call(layer, out_shape=pltpu.VMEM((TOK, W), BF16), in_specs=[hbm...  40.3 us

profile of v6, /device:TPU:1, one launch (start us, length us, event | category | flops | bytes accessed | tf_op | source)
XLA Modules:
  0.0 40.9 jit_solution(8774391820897807324)
XLA Ops:
  0.0 40.3 %layer.1 = bf16[16,512]{1,0:T(8,128)(2,1)S(1)} custom-call(bf16[16,512]{1,0:T(8,128)(2,1)} %tokens_hbm.1, s32[16]{0:T(128)} %lengths_hbm.1, f32[4]{0:T(128)} %bias_hbm.1, bf16[16,128]{1,0:T(8,128)(2,1)} %bitcast.17, bf16[16,128]{1,0:T(8,128)(2,1)} %bitcast.18, bf16[16,128]{1,0:T(8,128)(2,1)} %bitcast.19, s32[2,16]{1,0:T(2,128)} %bitcast.20, ...), custom_call_target="tpu_custom_call" | custom-call | tf_op jit(solution)/shard_map/layer/pallas_call | solution.py:777
  40.3 0.6 %copy.23 = bf16[16,512]{1,0:T(8,128)(2,1)} copy(bf16[16,512]{1,0:T(8,128)(2,1)S(1)} %layer.1) | data formatting | bytes 32768
